TPU v7x, 32 devices: a whole 2x2x4 slice. The times are simulated.
32 devices in a mesh: kv: 8 (over z, y), tp: 4 (over x, core).
Axes of the slice: x: 2, y: 2, z: 4, core: 2. Of those that a mesh axis runs over, the one named last changes fastest.
Arguments:
- piece_tokens: bfloat16 [1024, 4096], P('kv'), may hold values from -6 to 6
- decode_tokens: bfloat16 [8, 4096], P('kv'), may hold values from -6 to 6
- norm_gain: bfloat16 [4096], replicated, may hold values from 0.099609375 to 1.8984375
- w_query: bfloat16 [4096, 2048], P(None, 'tp'), may hold values from -0.09375 to 0.09375
- w_key: bfloat16 [4096, 2048], P(None, 'tp'), may hold values from -0.09375 to 0.09375
- w_value: bfloat16 [4096, 2048], P(None, 'tp'), may hold values from -0.09375 to 0.09375
- score_offset: float32 [16], replicated, may hold values from -14 to -3
- context_length: int32 [1], replicated, may hold values from 4096 to 8192
- prompt_keys: bfloat16 [8192, 2048], P('kv', 'tp'), may hold values from -16 to 16, as said below
- prompt_values: bfloat16 [8192, 2048], P('kv', 'tp'), may hold values from -6 to 6
- decode_keys: bfloat16 [8, 1024, 2048], P('kv', None, 'tp'), may hold values from -6 to 6
- decode_values: bfloat16 [8, 1024, 2048], P('kv', None, 'tp'), may hold values from -6 to 6
- decoding_cache_length: int32 [8], P('kv'), may hold values from 1 to 1024, as said below
- out_gain: bfloat16 [2048], replicated, may hold values from 0.099609375 to 1.8984375
- w_out: bfloat16 [2048, 4096], P(None, 'tp'), may hold values from -0.125 to 0.125
Outputs:
- prompt_piece_output: bfloat16 [1024, 4096], P('kv', 'tp')
- decode_out: bfloat16 [8, 4096], P('kv', 'tp')
- piece_keys: bfloat16 [1024, 2048], P('kv', 'tp')
- piece_values: bfloat16 [1024, 2048], P('kv', 'tp')
- decode_new_keys: bfloat16 [8, 2048], P('kv', 'tp')
- decode_new_values: bfloat16 [8, 2048], P('kv', 'tp')
Inputs may be any that keep to these rules, and one draw needn't show every extreme that they name: `prompt_keys`: the largest scale of a block of 1024 positions is up to four times the smallest. `decoding_cache_length`: some sequence has exactly 1024 valid positions.
All inputs are finite; a program needn't handle non-finite values.
Results may differ from a plain program's by a relative error of at most 0.008.
The roundings to bfloat16 on the way count: a program that leaves them out, or rounds other values in their place, can miss the bound.
Values may be sent and summed in bfloat16 or wider, within the bound.
A program may use at most 128 MiB of HBM per device.

v0:
```python
import functools

import jax
import jax.numpy as jnp
from jax import lax
from jax.experimental import pallas as pl
from jax.experimental.pallas import tpu as pltpu
from jax.sharding import PartitionSpec as P

HEAD = 128
EPS = 1e-06
HIDDEN = -1e30
MESH = pl.DeviceIdType.MESH


def rms_scaled(rows, gain):
    values = rows.astype(jnp.float32)
    inverse = lax.rsqrt(jnp.mean(values * values, axis=-1, keepdims=True) + EPS)
    return values * inverse * gain.astype(jnp.float32)


def suffix_matrix(size):
    row = lax.broadcasted_iota(jnp.int32, (size, size), 0)
    column = lax.broadcasted_iota(jnp.int32, (size, size), 1)
    return jnp.where(row >= column, 1.0, 0.0).astype(jnp.bfloat16)


def dot_t(a, b):
    return lax.dot_general(a, b, (((1,), (1,)), ((), ())), preferred_element_type=jnp.float32)


def dot(a, b):
    return jnp.dot(a, b, preferred_element_type=jnp.float32)


def suffix_keep(z, suffix):
    keep = -(jnp.maximum(z, 0.0) + jnp.log(1.0 + jnp.exp(-jnp.abs(z))))
    high = keep.astype(jnp.bfloat16)
    low = (keep - high.astype(jnp.float32)).astype(jnp.bfloat16)
    return dot(high, suffix) + dot(low, suffix)


def cached_terms(query, key_of, value_of, bias_of, total_keys, chunk, suffix, scale):
    later = None
    out = None
    for start in reversed(range(0, total_keys, chunk)):
        z = dot_t(query, key_of(start)) * scale + bias_of(start)
        inner = suffix_keep(z, suffix)
        exponent = z + inner if later is None else z + inner + later
        weight = jnp.exp(exponent).astype(jnp.bfloat16)
        part = dot(weight, value_of(start))
        out = part if out is None else out + part
        later = inner[:, 0:1] if later is None else later + inner[:, 0:1]
    return out, later


def attention_kernel(
    n, tp, heads, q_ref, k_ref, v_ref, dq_ref, ck_ref, cv_ref, cbias_ref, off_ref, dk_ref, dv_ref,
    dbias_ref, gain_ref, out_ref, qg, osend, orecv, psend, precv, tsend, trecv, ptot, later_s, att, attg,
    q_ss, q_rs, p_ss, p_rs, o_ss, o_rs, t_ss, t_rs, a_ss, a_rs,
):
    me = lax.axis_index("kv")
    mine = lax.axis_index("tp")
    rows = q_ref.shape[0]
    cache_rows = ck_ref.shape[0]
    seqs, slots = dk_ref.shape[0], dk_ref.shape[1]
    scale = HEAD ** (-0.5)
    chunk = 256 if cache_rows % 256 == 0 else 128

    barrier = pltpu.get_barrier_semaphore()
    for s in range(1, n):
        pl.semaphore_signal(barrier, inc=1, device_id={"kv": lax.rem(me + s, n)}, device_id_type=MESH)
    for s in range(1, tp):
        pl.semaphore_signal(barrier, inc=1, device_id={"tp": lax.rem(mine + s, tp)}, device_id_type=MESH)
    pl.semaphore_wait(barrier, n - 1 + tp - 1)

    def remote(src, dst, ss, rs, peer, axis="kv"):
        return pltpu.make_async_remote_copy(
            src_ref=src, dst_ref=dst, send_sem=ss, recv_sem=rs,
            device_id={axis: peer}, device_id_type=MESH,
        )

    def send_all(src, dst, ss, rs):
        for s in range(1, n):
            peer = lax.rem(me + n - s, n)
            remote(src, dst.at[me], ss.at[s], rs.at[me], peer).start()

    send_all(q_ref, qg, q_ss, q_rs)
    qg[me] = q_ref[...]

    wide = suffix_matrix(chunk)
    width = heads * HEAD
    hrow = lax.broadcasted_iota(jnp.int32, (8, width), 0)
    hcol = lax.broadcasted_iota(jnp.int32, (8, width), 1) // HEAD
    own_head = hrow == hcol
    att[pl.ds(rows, 16), :] = jnp.zeros((16, width), att.dtype)
    dec_rows = jnp.zeros((16, width), jnp.float32)
    for b in range(seqs):
        query = jnp.where(own_head, dq_ref[b : b + 1, :].astype(jnp.float32), 0.0).astype(jnp.bfloat16)
        out, unused = cached_terms(
            query,
            lambda start: dk_ref[b, pl.ds(start, chunk), :],
            lambda start: dv_ref[b, pl.ds(start, chunk), :],
            lambda start: dbias_ref[b, :, pl.ds(start, chunk)],
            slots, chunk, wide, scale,
        )
        row = jnp.sum(jnp.where(own_head, out, 0.0), axis=0, keepdims=True)
        place = lax.broadcasted_iota(jnp.int32, (16, width), 0)
        dec_rows = jnp.where(place == b, row, dec_rows)
    att[pl.ds(rows, 16), :] = dec_rows.astype(att.dtype)

    lane = lax.broadcasted_iota(jnp.int32, (rows, 128), 1)
    narrow = suffix_matrix(rows)
    qrow = lax.broadcasted_iota(jnp.int32, (rows, rows), 0)
    kcol = lax.broadcasted_iota(jnp.int32, (rows, rows), 1)
    for c in range(n):

        @pl.when(c > me)
        def _():
            precv[c] = jnp.zeros((rows, width), jnp.bfloat16)


    def block(s, carry):
        owner = lax.rem(me + s, n)

        @pl.when(s > 0)
        def _():
            remote(q_ref, qg.at[owner], q_ss.at[s], q_rs.at[owner], owner).wait_recv()

        totals = jnp.zeros((rows, 128), jnp.float32)
        for h in range(heads):
            cols = pl.ds(h * HEAD, HEAD)
            out, total = cached_terms(
                qg[owner, :, cols],
                lambda start: ck_ref[pl.ds(start, chunk), cols],
                lambda start: cv_ref[pl.ds(start, chunk), cols],
                lambda start: cbias_ref[h : h + 1, pl.ds(start, chunk)],
                cache_rows, chunk, wide, scale,
            )
            osend[owner, :, cols] = out.astype(jnp.bfloat16)
            totals = jnp.where(lane == h, total, totals)
        ptot[...] = totals

        @pl.when(owner >= me)
        def _():
            seen = (me * rows + kcol) < (owner * rows + qrow)
            totals = ptot[...]
            for h in range(heads):
                cols = pl.ds(h * HEAD, HEAD)
                z = dot_t(qg[owner, :, cols], k_ref[:, cols]) * scale + off_ref[h : h + 1, 0:1]
                z = jnp.where(seen, z, HIDDEN)
                inner = suffix_keep(z, narrow)
                weight = jnp.exp(z + inner).astype(jnp.bfloat16)
                psend[owner, :, cols] = dot(weight, v_ref[:, cols]).astype(jnp.bfloat16)
                totals = jnp.where(lane == heads + h, inner[:, 0:1], totals)
            ptot[...] = totals

        tsend[owner] = jnp.transpose(ptot[...])[0:8, :]

        @pl.when(s > 0)
        def _():
            place = pl.ds(pl.multiple_of(me * 8, 8), 8)
            remote(tsend.at[owner], trecv.at[place], t_ss.at[s], t_rs.at[me], owner).start()
            remote(osend.at[owner], orecv.at[me], o_ss.at[s], o_rs.at[me], owner).start()

        @pl.when(owner > me)
        def _():
            remote(psend.at[owner], precv.at[me], p_ss.at[s], p_rs.at[me], owner).start()

        return carry

    lax.fori_loop(0, n, block, 0)
    orecv[me] = osend[me]
    precv[me] = psend[me]
    trecv[pl.ds(pl.multiple_of(me * 8, 8), 8), :] = tsend[me]

    for s in range(1, n):
        peer = lax.rem(me + s, n)
        place = pl.ds(pl.multiple_of(peer * 8, 8), 8)
        remote(tsend.at[peer], trecv.at[place], t_ss.at[s], t_rs.at[peer], peer).wait()
        remote(osend.at[peer], orecv.at[peer], o_ss.at[s], o_rs.at[peer], peer).wait()
        remote(q_ref, qg.at[peer], q_ss.at[s], q_rs.at[peer], peer).wait_send()
        pieces = remote(psend.at[peer], precv.at[peer], p_ss.at[s], p_rs.at[peer], peer)

        @pl.when(peer > me)
        def _():
            pieces.wait_send()

        @pl.when(peer < me)
        def _():
            pieces.wait_recv()

    run = jnp.zeros((8, 128), jnp.float32)
    later_s[...] = jnp.zeros_like(later_s)
    for c in reversed(range(n)):
        later_s[c * 8 : c * 8 + 8, :] = run
        run = run + trecv[c * 8 : c * 8 + 8, :]
    later_s[n * 8 : n * 8 + 8, :] = run
    factors = [
        jnp.exp(jnp.transpose(later_s[g * 128 : g * 128 + 128, :]))
        for g in range(later_s.shape[0] // 128)
    ]

    def factor(c, row):
        group, spot = divmod(c * 8 + row, 128)
        return factors[group][:, spot : spot + 1]

    for h in range(heads):
        cols = pl.ds(h * HEAD, HEAD)
        mixed = jnp.zeros((rows, HEAD), jnp.float32)
        pieces = jnp.zeros((rows, HEAD), jnp.float32)
        for c in range(n):
            mixed += orecv[c, :, cols].astype(jnp.float32) * factor(c, h)
            pieces += precv[c, :, cols].astype(jnp.float32) * factor(c, heads + h)
        mixed = mixed * factor(n, heads + h) + pieces
        att[pl.ds(0, rows), cols] = mixed.astype(att.dtype)

    for s in range(1, tp):
        peer = lax.rem(mine + s, tp)
        remote(att, attg.at[mine], a_ss.at[s], a_rs.at[mine], peer, "tp").start()
    attg[mine] = att[...]
    for s in range(1, tp):
        peer = lax.rem(mine + s, tp)
        remote(att, attg.at[peer], a_ss.at[s], a_rs.at[peer], peer, "tp").wait()
    square = jnp.zeros((att.shape[0], 1), jnp.float32)
    for t in range(tp):
        values = attg[t].astype(jnp.float32)
        square += jnp.sum(values * values, axis=-1, keepdims=True)
    inverse = lax.rsqrt(square / (tp * width) + EPS)
    for t in range(tp):
        cols = pl.ds(t * width, width)
        gain = gain_ref[0:1, cols].astype(jnp.float32)
        out_ref[:, cols] = (attg[t].astype(jnp.float32) * inverse * gain).astype(out_ref.dtype)


def body(
    piece_tokens, decode_tokens, norm_gain, w_query, w_key, w_value, score_offset, context_length,
    prompt_keys, prompt_values, decode_keys, decode_values, decoding_cache_length, out_gain, w_out,
):
    n, tp = lax.axis_size("kv"), lax.axis_size("tp")
    width = w_query.shape[1]
    heads = width // HEAD
    offset = lax.dynamic_slice_in_dim(score_offset, lax.axis_index("tp") * heads, heads)
    offset = jnp.pad(offset, (0, 8 - heads))
    rows = piece_tokens.shape[0]
    all_rows = jnp.concatenate([piece_tokens, decode_tokens], axis=0)
    normed_in = rms_scaled(all_rows, norm_gain).astype(jnp.bfloat16)
    queries = jnp.dot(normed_in, w_query, preferred_element_type=jnp.float32).astype(jnp.bfloat16)
    new_keys = jnp.dot(normed_in, w_key, preferred_element_type=jnp.float32).astype(jnp.bfloat16)
    new_values = jnp.dot(normed_in, w_value, preferred_element_type=jnp.float32).astype(
        jnp.bfloat16
    )
    cache_rows = prompt_keys.shape[0]
    seqs, slots = decode_keys.shape[:2]
    places = lax.axis_index("kv") * cache_rows + jnp.arange(cache_rows, dtype=jnp.int32)
    cache_bias = jnp.where(places[None, :] < context_length[0], offset[:, None], HIDDEN)
    spots = jnp.arange(slots, dtype=jnp.int32)[None, None, :]
    decode_bias = jnp.where(
        spots < decoding_cache_length[:, None, None], offset[None, :, None], HIDDEN
    )
    wide_offset = jnp.broadcast_to(offset[:, None], (8, 128))
    trows = -(-(n + 1) * 8 // 128) * 128
    vmem = pl.BlockSpec(memory_space=pltpu.VMEM)
    dma = pltpu.SemaphoreType.DMA
    block = pltpu.VMEM((n, rows, width), jnp.bfloat16)
    normed_out = pl.pallas_call(
        functools.partial(attention_kernel, n, tp, heads),
        out_shape=jax.ShapeDtypeStruct((rows + 16, tp * width), jnp.bfloat16),
        in_specs=[vmem] * 12,
        out_specs=vmem,
        scratch_shapes=[
            block, block, block, block, block,
            pltpu.VMEM((n, 8, 128), jnp.float32),
            pltpu.VMEM((trows, 128), jnp.float32),
            pltpu.VMEM((rows, 128), jnp.float32),
            pltpu.VMEM((trows, 128), jnp.float32),
            pltpu.VMEM((rows + 16, width), jnp.bfloat16),
            pltpu.VMEM((tp, rows + 16, width), jnp.bfloat16),
        ] + [dma((n,)) for _ in range(8)] + [dma((tp,)), dma((tp,))],
        compiler_params=pltpu.CompilerParams(
            collective_id=0, has_side_effects=True, vmem_limit_bytes=56 * 1024 * 1024
        ),
        name="attend",
    )(
        queries[:rows], new_keys[:rows], new_values[:rows], queries[rows:], prompt_keys,
        prompt_values, cache_bias, wide_offset, decode_keys, decode_values, decode_bias,
        out_gain[None, :],
    )
    outputs = jnp.dot(normed_out, w_out, preferred_element_type=jnp.float32).astype(jnp.bfloat16)
    return (
        outputs[:rows],
        outputs[rows : rows + seqs],
        new_keys[:rows],
        new_values[:rows],
        new_keys[rows:],
        new_values[rows:],
    )


def solution(mesh):
    in_specs = (
        P("kv", None),
        P("kv", None),
        P(),
        P(None, "tp"),
        P(None, "tp"),
        P(None, "tp"),
        P(),
        P(),
        P("kv", "tp"),
        P("kv", "tp"),
        P("kv", None, "tp"),
        P("kv", None, "tp"),
        P("kv"),
        P(),
        P(None, "tp"),
    )
    out_specs = (
        P("kv", "tp"),
        P("kv", "tp"),
        P("kv", "tp"),
        P("kv", "tp"),
        P("kv", "tp"),
        P("kv", "tp"),
    )
    return jax.shard_map(body, mesh=mesh, in_specs=in_specs, out_specs=out_specs, check_vma=False)
```

profile of v0, /device:TPU:9, one launch (start us, length us, event | category | flops | bytes accessed | tf_op | source)
XLA Modules:
  0.0 105.1 jit_solution(18211609830521121482)
XLA Ops:
  1.9 0.7 dynamic_slice.3
  2.7 1.6 %fusion = f32[129]{0:T(256)S(1)} fusion(bf16[1,4096]{1,0:T(2,128)(2,1)} %param.16, bf16[128,4096]{1,0:T(8,128)(2,1)} %param.15), kind=kLoop, calls=%fused_computation.2 | loop fusion | flops 3170175 | bytes 1057284 | tf_op jit(solution)/shard_map/reduce_sum | solution.py:18
  4.3 0.7 broadcast_in_dim.59.off_ref
  4.9 1.3 %broadcast_in_dim.63.gain_ref = bf16[1,2048]{1,0:T(2,128)(2,1)} reshape(bf16[2048]{0:T(1024)(128)(2,1)} %param.28) | data formatting | bytes 8192 | tf_op jit(solution)/shard_map/broadcast_in_dim | solution.py:287
  6.2 0.7 convert_element_type.24
  6.9 0.7 broadcast_select_fusion.dbias_ref
  7.6 0.7 broadcast_select_fusion.1.cbias_ref
  8.3 0.0 copy-start.1
  8.3 0.0 copy-start.2
  8.3 0.0 copy-start.3
  8.3 3.5 %convolution_convert_fusion.2 = bf16[129,512]{1,0:T(8,128)(2,1)S(1)} fusion(bf16[4096,512]{1,0:T(8,128)(2,1)} %param.19, f32[4096]{0:T(1024)S(1)} %convert_element_type.24, f32[129]{0:T(256)S(1)} %add_rsqrt_fusion, bf16[1,4096]{1,0:T(2,128)(2,1)} %param.16, bf16[128,4096]{1,0:T(8,128)(2,1)} %param.15), kind=kOutput, calls=%fused_computation.7 | convolution fusion | flops 544829952 | bytes 5400068 | tf_op jit(solution)/shard_map/dot_general | solution.py:249
  11.7 0.6 slice.40
  12.3 0.7 slice.35.k_ref
  13.0 0.0 copy-done.1
  13.0 0.0 copy-done.2
  13.0 0.0 copy-done.3
  13.0 0.0 copy-start.4
  13.0 0.8 convolution_convert_fusion.1
  13.8 0.6 slice.41
  14.4 0.7 slice.36.v_ref
  15.1 0.1 copy-done.4
  15.2 0.8 convolution_convert_fusion.3
  16.0 0.6 slice.37.dq_ref
  16.6 0.7 slice.34.q_ref
  17.2 0.0 copy-start
  17.2 84.6 %attend.1 = bf16[144,2048]{1,0:T(8,128)(2,1)} custom-call(bf16[128,512]{1,0:T(8,128)(2,1)} %slice.34.q_ref, bf16[128,512]{1,0:T(8,128)(2,1)} %slice.35.k_ref, bf16[128,512]{1,0:T(8,128)(2,1)} %slice.36.v_ref, bf16[1,512]{1,0:T(2,128)(2,1)} %slice.37.dq_ref, bf16[1024,512]{1,0:T(8,128)(2,1)} %ck_ref.1, bf16[1024,512]{1,0:T(8,128)(2,1)} %cv_ref.1, ...), custom_call_target="tpu_custom_call" | custom-call | tf_op jit(solution)/shard_map/attend/pallas_call | solution.py:266
  101.9 0.0 copy-done
  101.9 1.8 %convolution_convert_fusion = bf16[144,1024]{1,0:T(8,128)(2,1)S(1)} fusion(bf16[144,2048]{1,0:T(8,128)(2,1)} %attend.1, bf16[2048,1024]{1,0:T(8,128)(2,1)S(1)} %copy-done), kind=kOutput, calls=%fused_computation.5 | convolution fusion | flops 604127232 | bytes 5079040 | tf_op jit(solution)/shard_map/dot_general | solution.py:289
  103.7 0.6 slice.39
  104.3 0.7 slice.38
  (4 shorter events, 0.0 us)
Async XLA Ops:
  8.3 4.7 %copy-start.1 = (bf16[128,4096]{1,0:T(8,128)(2,1)S(1)}, bf16[128,4096]{1,0:T(8,128)(2,1)}, u32[]{:S(2)}) copy-start(bf16[128,4096]{1,0:T(8,128)(2,1)} %param.15) | copy-start | bytes 3145732
  8.3 4.7 %copy-start.2 = (bf16[1,4096]{1,0:T(2,128)(2,1)S(1)}, bf16[1,4096]{1,0:T(2,128)(2,1)}, u32[]{:S(2)}) copy-start(bf16[1,4096]{1,0:T(2,128)(2,1)} %param.16) | copy-start | bytes 24580
  8.3 4.7 %copy-start.3 = (bf16[4096,512]{1,0:T(8,128)(2,1)S(1)}, bf16[4096,512]{1,0:T(8,128)(2,1)}, u32[]{:S(2)}) copy-start(bf16[4096,512]{1,0:T(8,128)(2,1)} %param.20) | copy-start | bytes 12582916
  13.0 2.2 %copy-start.4 = (bf16[4096,512]{1,0:T(8,128)(2,1)S(1)}, bf16[4096,512]{1,0:T(8,128)(2,1)}, u32[]{:S(2)}) copy-start(bf16[4096,512]{1,0:T(8,128)(2,1)} %param.18) | copy-start | bytes 12582916
  17.2 84.7 %copy-start = (bf16[2048,1024]{1,0:T(8,128)(2,1)S(1)}, bf16[2048,1024]{1,0:T(8,128)(2,1)}, u32[]{:S(2)}) copy-start(bf16[2048,1024]{1,0:T(8,128)(2,1)} %param.29) | copy-start | bytes 12582916
where the time goes:
time: 106 us; the launch traced here: 105 us
  Pallas kernels  84.6 us (80%)
  local copies, waits for them, and re-layouts  7.92 us (7%)
  matrix products  6.87 us (6%)
  other arithmetic  3.63 us (3%)
  between operations  2 us (2%)
    pallas_call x1, Pallas kernels, body(): pl.pallas_call(functools.partial(attention_kernel, n, tp, heads), out_sha...  84.6 us
    dot_general x1, matrix products, body(): jnp.dot(normed_in, w_key, preferred_element_type=jnp.float32)  3.46 us

commit v1 on v0

v1 whole, which is shorter than its diff:
```python
import functools
import math

import jax
import jax.numpy as jnp
from jax import lax
from jax.experimental import pallas as pl
from jax.experimental.pallas import tpu as pltpu
from jax.sharding import PartitionSpec as P

HEAD = 128
EPS = 1e-06
HIDDEN = -1e30
LOG2E = 1.4426950408889634
MESH = pl.DeviceIdType.MESH


def rms_scaled(rows, gain):
    values = rows.astype(jnp.float32)
    inverse = lax.rsqrt(jnp.mean(values * values, axis=-1, keepdims=True) + EPS)
    return values * inverse * gain.astype(jnp.float32)


def suffix_matrix(size):
    row = lax.broadcasted_iota(jnp.int32, (size, size), 0)
    column = lax.broadcasted_iota(jnp.int32, (size, size), 1)
    return jnp.where(row >= column, 1.0, 0.0).astype(jnp.bfloat16)


def spread_matrix(size):
    run = size // 8
    row = lax.broadcasted_iota(jnp.int32, (size, size), 0)
    column = lax.broadcasted_iota(jnp.int32, (size, size), 1)
    hit = (row // 8 == column % run) & (row % 8 == column // run)
    return jnp.where(hit, 1.0, 0.0).astype(jnp.bfloat16)


def dot_t(a, b):
    return lax.dot_general(a, b, (((1,), (1,)), ((), ())), preferred_element_type=jnp.float32)


def dot(a, b):
    return jnp.dot(a, b, preferred_element_type=jnp.float32)


def suffix_keep(z, suffix):
    keep = -(jnp.maximum(z, 0.0) + jnp.log(1.0 + jnp.exp(-jnp.abs(z))))
    high = keep.astype(jnp.bfloat16)
    low = (keep - high.astype(jnp.float32)).astype(jnp.bfloat16)
    return dot(high, suffix) + dot(low, suffix)


def cached_terms(query, key_of, value_of, bias_of, total_keys, chunk, suffix, scale):
    later = None
    out = None
    for start in reversed(range(0, total_keys, chunk)):
        z = dot_t(query, key_of(start)) * scale + bias_of(start)
        inner = suffix_keep(z, suffix)
        exponent = z + inner if later is None else z + inner + later
        weight = jnp.exp(exponent).astype(jnp.bfloat16)
        part = dot(weight, value_of(start))
        out = part if out is None else out + part
        later = inner[:, 0:1] if later is None else later + inner[:, 0:1]
    return out, later


def grid_of(n):
    columns = max(d for d in range(1, math.isqrt(n) + 1) if n % d == 0)
    return n // columns, columns


def later_sublanes(runs):
    place = lax.broadcasted_iota(jnp.int32, runs.shape, 0)

    def up(x, k):
        return jnp.where(place < 8 - k, pltpu.roll(x, 8 - k, 0), 1.0)

    x = up(runs, 1)
    x = x * up(x, 1)
    x = x * up(x, 2)
    return x * up(x, 4)


def break_sticks(score, store, steps, groups):
    left = [jnp.ones((8, 128), jnp.float32) for _ in range(groups)]
    for v in reversed(range(steps)):
        for g in range(groups):
            e = jnp.exp2(jnp.minimum(score(v, g), 126.0))
            left[g] = left[g] * (1.0 / (1.0 + e))
            store(v, g, e * left[g])
    return left


def attention_kernel(
    nz, ny, tp, heads, q_ref, k_ref, v_ref, dq_ref, ck_ref, cv_ref, dk_ref, dv_ref, gain_ref, off_ref,
    ctx_ref, len_ref, out_ref,
    qg, kp, vt, tab, zbuf, own, obuf, tbuf, oy, ty, mix, zs, zt, zr, ztr, zmix,
    kvb, kvg, qp, pz, pacc, plat, ps, pt, pr, ptr, att, attg,
    q_ys, q_zs, q_fs, q_rs, kv_zs, kv_ys, kv_fs, kv_rs, oy_s, oy_r, ty_s, ty_r, oz_s, oz_r, tz_s, tz_r,
    p_s, p_r, pt_s, pt_r, a_s, a_r,
):
    n = nz * ny
    me = lax.axis_index("kv")
    mine = lax.axis_index("tp")
    z = me // ny
    y = lax.rem(me, ny)
    rows = q_ref.shape[0]
    width = heads * HEAD
    cache_rows = ck_ref.shape[0]
    seqs, slots = dk_ref.shape[0], dk_ref.shape[1]
    scale = HEAD ** (-0.5)
    scale2 = scale * LOG2E
    halves = nz // heads
    my_head = lax.rem(z, heads)
    my_part = z // heads
    bits = nz.bit_length() - 1
    paired = nz == 1 << bits

    def turned(s):
        total = 0
        for b in range(bits):
            total += lax.rem(lax.rem(z // (1 << b), 2) + lax.rem(s // (1 << b), 2), 2) * (1 << b)
        return total

    def source(s):
        return turned(s) if paired else lax.rem(z + s, nz)

    def target(s):
        return turned(s) if paired else lax.rem(z + nz - s, nz)

    def other(k):
        return lax.rem(y + k, ny)

    def head_cols(h):
        return pl.ds(h * HEAD, HEAD)

    barrier = pltpu.get_barrier_semaphore()
    for s in range(1, n):
        pl.semaphore_signal(barrier, inc=1, device_id={"kv": lax.rem(me + s, n)}, device_id_type=MESH)
    for s in range(1, tp):
        pl.semaphore_signal(barrier, inc=1, device_id={"tp": lax.rem(mine + s, tp)}, device_id_type=MESH)
    pl.semaphore_wait(barrier, n - 1 + tp - 1)

    def remote(src, dst, ss, rs, peer, axis="kv"):
        return pltpu.make_async_remote_copy(
            src_ref=src, dst_ref=dst, send_sem=ss, recv_sem=rs,
            device_id={axis: peer}, device_id_type=MESH,
        )

    def q_plane(s):
        return remote(q_ref, qg.at[me], q_zs.at[s], q_rs.at[me], target(s) * ny + y)

    def q_column(k):
        return remote(q_ref, qg.at[me], q_ys.at[k], q_rs.at[me], z * ny + other(k))

    def q_block(c, s, k):
        return remote(qg.at[c], qg.at[c], q_fs.at[s, k], q_rs.at[c], z * ny + other(k))

    for s in range(1, nz):
        q_plane(s).start()
    for k in range(1, ny):
        q_column(k).start()
    qg[me] = q_ref[...]

    short = spread_matrix(rows)
    for h in range(heads):
        kvb[h, 0:rows, :] = dot(short, k_ref[:, head_cols(h)]).astype(jnp.bfloat16)
        kvb[h, rows : 2 * rows, :] = jnp.transpose(dot(short, v_ref[:, head_cols(h)])).astype(jnp.bfloat16)

    def kv_plane(t):
        return remote(kvb.at[t % heads], kvg.at[me], kv_zs.at[t], kv_rs.at[me], t * ny + y)

    def kv_column(k):
        return remote(kvb.at[my_head], kvg.at[me], kv_ys.at[k], kv_rs.at[me], z * ny + other(k))

    def kv_block(c, s, k):
        return remote(kvg.at[c], kvg.at[c], kv_fs.at[s, k], kv_rs.at[c], z * ny + other(k))

    for t in range(nz):
        pl.when(z != t)(lambda t=t: kv_plane(t).start())
    for k in range(1, ny):
        kv_column(k).start()
    kvg[me] = kvb[my_head]

    run = cache_rows // 8
    tiles = run // 32
    wide = spread_matrix(256)
    for t in range(tiles):
        def strip(ref):
            return jnp.concatenate([ref[pl.ds(s * run + t * 32, 32), :] for s in range(8)], axis=0)
        keys = dot(wide, strip(ck_ref)).astype(jnp.bfloat16)
        values = dot(wide, strip(cv_ref))
        for h in range(heads):
            kp[h, t * 256 : t * 256 + 256, :] = keys[:, h * HEAD : h * HEAD + HEAD]
            vt[h, :, t * 256 : t * 256 + 256] = jnp.transpose(
                values[:, h * HEAD : h * HEAD + HEAD]
            ).astype(jnp.bfloat16)
    row = lax.broadcasted_iota(jnp.int32, (cache_rows, 128), 0)
    valid = me * cache_rows + lax.rem(row, 8) * run + row // 8 < ctx_ref[0]
    for h in range(heads):
        tab[h] = jnp.where(valid, off_ref[mine * heads + h] * LOG2E, HIDDEN)

    chunk = 256 if slots % 256 == 0 else 128
    suffix = suffix_matrix(chunk)
    hrow = lax.broadcasted_iota(jnp.int32, (8, width), 0)
    hcol = lax.broadcasted_iota(jnp.int32, (8, width), 1) // HEAD
    own_head = hrow == hcol
    head_row = lax.broadcasted_iota(jnp.int32, (8, chunk), 0)
    spot = lax.broadcasted_iota(jnp.int32, (8, chunk), 1)
    offsets = jnp.zeros((8, chunk), jnp.float32)
    for h in range(heads):
        offsets = jnp.where(head_row == h, off_ref[mine * heads + h], offsets)
    dec_rows = jnp.zeros((16, width), jnp.float32)
    for b in range(seqs):
        query = jnp.where(own_head, dq_ref[b : b + 1, :].astype(jnp.float32), 0.0).astype(jnp.bfloat16)
        out, unused = cached_terms(
            query,
            lambda start: dk_ref[b, pl.ds(start, chunk), :],
            lambda start: dv_ref[b, pl.ds(start, chunk), :],
            lambda start: jnp.where(spot + start < len_ref[b], offsets, HIDDEN),
            slots, chunk, suffix, scale,
        )
        line = jnp.sum(jnp.where(own_head, out, 0.0), axis=0, keepdims=True)
        place = lax.broadcasted_iota(jnp.int32, (16, width), 0)
        dec_rows = jnp.where(place == b, line, dec_rows)
    att[pl.ds(rows, 16), :] = dec_rows.astype(att.dtype)

    def forward(s):
        c = source(s) * ny + y
        q_block(c, s, 0).wait_recv()
        kv_block(c, s, 0).wait_recv()
        for k in range(1, ny):
            q_block(c, s, k).start()
            kv_block(c, s, k).start()

    def piece_out(j):
        return remote(ps.at[j], pr.at[my_head], p_s.at[j], p_r.at[my_head], (my_part + halves * j) * ny + y)

    def piece_total(j):
        return remote(pt.at[j], ptr.at[my_head], pt_s.at[j], pt_r.at[my_head], (my_part + halves * j) * ny + y)

    def pieces():
        for k in range(1, ny):
            for u in range(nz):
                kv_block(u * ny + other(k), 0, 0).wait_recv()
        cols = pl.ds(pl.multiple_of(my_head * HEAD, HEAD), HEAD)
        for j in range(heads):
            qp[j * rows : j * rows + rows, :] = qg[(my_part + halves * j) * ny + y, :, cols]
        pacc[...] = jnp.zeros_like(pacc)
        plat[...] = jnp.ones_like(plat)
        lane = lax.broadcasted_iota(jnp.int32, (8, 128), 1)
        first = lax.broadcasted_iota(jnp.int32, (8, 128), 0) * (rows // 8)
        off = off_ref[mine * heads + my_head] * LOG2E

        def block(i, carry):
            c = n - 1 - i
            pz[...] = dot_t(kvg[c, 0:rows, :], qp[...])

            def score(v, g):
                seen = c * rows + first + v < ((my_part + halves * g) * ny + y) * rows + lane
                return jnp.where(seen, pz[v * 8 : v * 8 + 8, g * 128 : g * 128 + 128] * scale2 + off, HIDDEN)

            def store(v, g, w):
                pz[v * 8 : v * 8 + 8, g * 128 : g * 128 + 128] = w

            left = break_sticks(score, store, rows // 8, heads)
            factors = [later_sublanes(x) for x in left]
            factor = jnp.concatenate(factors, axis=1)
            w = pz[...].reshape(rows // 8, 8, heads * rows) * factor[None]
            w = w.reshape(rows, heads * rows).astype(jnp.bfloat16)
            pacc[...] += dot(kvg[c, rows : 2 * rows, :], w) * plat[0:1, :]
            whole = (factor * jnp.concatenate(left, axis=1))[0:1, :]
            plat[...] = plat[...] * whole
            return carry

        lax.fori_loop(0, n, block, 0)
        for j in range(heads):
            owner = my_part + halves * j
            ps[j] = pacc[:, j * rows : j * rows + rows].astype(jnp.bfloat16)
            pt[j] = plat[:, j * rows : j * rows + rows]

            @pl.when(owner != z)
            def _():
                piece_out(j).start()
                piece_total(j).start()

            @pl.when(owner == z)
            def _():
                pr[my_head] = ps[j]
                ptr[my_head] = pt[j]

    def o_column(u, s, k):
        return remote(obuf.at[u, other(k)], oy.at[u, y], oy_s.at[s, k], oy_r.at[u, y], z * ny + other(k))

    def t_column(u, s, k):
        return remote(tbuf.at[u, other(k)], ty.at[u, y], ty_s.at[s, k], ty_r.at[u, y], z * ny + other(k))

    def o_from(u, c):
        return remote(obuf.at[u, c], oy.at[u, c], oy_s.at[0, 0], oy_r.at[u, c], z * ny + other(1))

    def t_from(u, c):
        return remote(tbuf.at[u, c], ty.at[u, c], ty_s.at[0, 0], ty_r.at[u, c], z * ny + other(1))

    def compute(u):
        totals = [jnp.ones((8, 128), jnp.float32) for _ in range(ny)]
        place = lax.broadcasted_iota(jnp.int32, (8, 128), 0)
        for h in range(heads):
            q = qg[pl.ds(u * ny, ny), :, head_cols(h)].reshape(ny * rows, HEAD)
            zbuf[h] = dot_t(kp[h], q)

            def score(v, g):
                at = slice(v * 8, v * 8 + 8)
                return zbuf[h, at, g * 128 : g * 128 + 128] * scale2 + tab[h, at, :]

            def store(v, g, w):
                zbuf[h, v * 8 : v * 8 + 8, g * 128 : g * 128 + 128] = w

            left = break_sticks(score, store, run, ny)
            factors = [later_sublanes(x) for x in left]
            factor = jnp.concatenate(factors, axis=1)
            w = zbuf[h].reshape(run, 8, ny * rows) * factor[None]
            out = dot(vt[h], w.reshape(cache_rows, ny * rows).astype(jnp.bfloat16))
            for g in range(ny):
                part = out[:, g * rows : g * rows + rows]
                own[u, g, head_cols(h), :] = part
                obuf[u, g, head_cols(h), :] = part.astype(jnp.bfloat16)
                totals[g] = jnp.where(place == h, (factors[g] * left[g])[0:1, :], totals[g])
        for g in range(ny):
            tbuf[u, g] = totals[g]
        ty[u, y] = tbuf[u, y]

    def o_plane(u, s):
        return remote(zs.at[u], zr.at[z], oz_s.at[s], oz_r.at[z], u * ny + y)

    def t_plane(u, s):
        return remote(zt.at[u], ztr.at[z], tz_s.at[s], tz_r.at[z], u * ny + y)

    def combine(s):
        u = source(s)
        mix[y] = own[u, y]
        for k in range(1, ny):
            o_from(u, other(k)).wait_recv()
            t_from(u, other(k)).wait_recv()
            mix[other(k)] = oy[u, other(k)].astype(jnp.float32)
        later = jnp.ones((8, 128), jnp.float32)
        factors = []
        for c in reversed(range(ny)):
            factors.append(later)
            later = later * ty[u, c]
        for h in range(heads):
            total = jnp.zeros((HEAD, rows), jnp.float32)
            for c in range(ny):
                total += mix[c, head_cols(h), :] * factors[ny - 1 - c][h : h + 1, :]
            zs[u, head_cols(h), :] = total.astype(jnp.bfloat16)

            @pl.when(u == z)
            def _():
                zmix[z, head_cols(h), :] = total

        zt[u] = later

        @pl.when(u == z)
        def _():
            ztr[z] = later

        @pl.when(u != z)
        def _():
            o_plane(u, s).start()
            t_plane(u, s).start()

    def step(s, carry):
        u = source(s)
        pl.when(s + 1 < nz)(lambda: forward(s + 1))
        for k in range(1, ny):
            q_block(u * ny + other(k), 0, 0).wait_recv()
        pl.when(s == nz - 1)(pieces)
        compute(u)
        for k in range(1, ny):
            o_column(u, s, k).start()
            t_column(u, s, k).start()
        pl.when(s > 0)(lambda: combine(s - 1))
        return carry

    lax.fori_loop(0, nz, step, 0)
    combine(nz - 1)

    for h in range(heads):
        plane = lax.rem(z, halves) * heads + h

        @pl.when(plane != z)
        def _():
            remote(ps.at[0], pr.at[h], p_s.at[0], p_r.at[h], plane * ny + y).wait_recv()
            remote(pt.at[0], ptr.at[h], pt_s.at[0], pt_r.at[h], plane * ny + y).wait_recv()

    for s in range(1, nz):
        u = source(s)
        remote(zs.at[u], zr.at[u], oz_s.at[s], oz_r.at[u], u * ny + y).wait_recv()
        remote(zt.at[u], ztr.at[u], tz_s.at[s], tz_r.at[u], u * ny + y).wait_recv()
        zmix[u] = zr[u].astype(jnp.float32)

    later = jnp.ones((8, 128), jnp.float32)
    factors = []
    for c in reversed(range(nz)):
        factors.append(later)
        later = later * ztr[c]
    for h in range(heads):
        total = jnp.zeros((HEAD, rows), jnp.float32)
        for c in range(nz):
            total += zmix[c, head_cols(h), :] * factors[nz - 1 - c][h : h + 1, :]
        total = total * ptr[h, 0:1, :] + pr[h].astype(jnp.float32)
        att[pl.ds(0, rows), head_cols(h)] = jnp.transpose(total).astype(att.dtype)

    for s in range(1, tp):
        peer = lax.rem(mine + s, tp)
        remote(att, attg.at[mine], a_s.at[s], a_r.at[mine], peer, "tp").start()
    attg[mine] = att[...]

    for s in range(1, nz):
        q_plane(s).wait_send()
        u = source(s)
        c = u * ny + y
        o_plane(u, s).wait_send()
        t_plane(u, s).wait_send()
        for k in range(1, ny):
            q_block(c, s, k).wait_send()
            kv_block(c, s, k).wait_send()
    for t in range(nz):
        pl.when(z != t)(lambda t=t: kv_plane(t).wait_send())
    for k in range(1, ny):
        q_column(k).wait_send()
        kv_column(k).wait_send()
        for s in range(nz):
            o_column(source(s), s, k).wait_send()
            t_column(source(s), s, k).wait_send()
    for j in range(heads):

        @pl.when(my_part + halves * j != z)
        def _():
            piece_out(j).wait_send()
            piece_total(j).wait_send()

    for s in range(1, tp):
        peer = lax.rem(mine + s, tp)
        remote(att, attg.at[peer], a_s.at[s], a_r.at[peer], peer, "tp").wait()
    square = jnp.zeros((att.shape[0], 1), jnp.float32)
    for t in range(tp):
        values = attg[t].astype(jnp.float32)
        square += jnp.sum(values * values, axis=-1, keepdims=True)
    inverse = lax.rsqrt(square / (tp * width) + EPS)
    for t in range(tp):
        cols = pl.ds(t * width, width)
        gain = gain_ref[0:1, cols].astype(jnp.float32)
        out_ref[:, cols] = (attg[t].astype(jnp.float32) * inverse * gain).astype(out_ref.dtype)


def attend(
    nz, ny, tp, queries, keys, values, decode_queries, prompt_keys, prompt_values, decode_keys, decode_values,
    out_gain, score_offset, context_length, decoding_cache_length,
):
    n = nz * ny
    rows, width = queries.shape
    heads = width // HEAD
    assert nz % heads == 0
    cache_rows = prompt_keys.shape[0]
    vmem = pl.BlockSpec(memory_space=pltpu.VMEM)
    smem = pl.BlockSpec(memory_space=pltpu.SMEM)
    dma = pltpu.SemaphoreType.DMA

    def half(*shape):
        return pltpu.VMEM(shape, jnp.bfloat16)

    def full(*shape):
        return pltpu.VMEM(shape, jnp.float32)

    return pl.pallas_call(
        functools.partial(attention_kernel, nz, ny, tp, heads),
        out_shape=jax.ShapeDtypeStruct((rows + 16, tp * width), jnp.bfloat16),
        in_specs=[vmem] * 9 + [smem] * 3,
        out_specs=vmem,
        scratch_shapes=[
            half(n, rows, width), half(heads, cache_rows, HEAD), half(heads, HEAD, cache_rows),
            full(heads, cache_rows, 128), full(heads, cache_rows, ny * rows),
            full(nz, ny, width, rows), half(nz, ny, width, rows), full(nz, ny, 8, 128),
            half(nz, ny, width, rows), full(nz, ny, 8, 128), full(ny, width, rows),
            half(nz, width, rows), full(nz, 8, 128), half(nz, width, rows), full(nz, 8, 128),
            full(nz, width, rows),
            half(heads, 2 * rows, HEAD), half(n, 2 * rows, HEAD), half(heads * rows, HEAD),
            full(rows, heads * rows), full(HEAD, heads * rows), full(8, heads * rows),
            half(heads, HEAD, rows), full(heads, 8, 128), half(heads, HEAD, rows), full(heads, 8, 128),
            half(rows + 16, width), half(tp, rows + 16, width),
            dma((ny,)), dma((nz,)), dma((nz, ny)), dma((n,)),
            dma((nz,)), dma((ny,)), dma((nz, ny)), dma((n,)),
            dma((nz, ny)), dma((nz, ny)), dma((nz, ny)), dma((nz, ny)),
            dma((nz,)), dma((nz,)), dma((nz,)), dma((nz,)),
            dma((heads,)), dma((heads,)), dma((heads,)), dma((heads,)),
            dma((tp,)), dma((tp,)),
        ],
        compiler_params=pltpu.CompilerParams(
            collective_id=0, has_side_effects=True, vmem_limit_bytes=56 * 1024 * 1024
        ),
        name="attend",
    )(
        queries, keys, values, decode_queries, prompt_keys, prompt_values, decode_keys, decode_values,
        out_gain[None, :], score_offset, context_length, decoding_cache_length,
    )


def body(
    piece_tokens, decode_tokens, norm_gain, w_query, w_key, w_value, score_offset, context_length,
    prompt_keys, prompt_values, decode_keys, decode_values, decoding_cache_length, out_gain, w_out,
):
    n, tp = lax.axis_size("kv"), lax.axis_size("tp")
    nz, ny = grid_of(n)
    rows = piece_tokens.shape[0]
    seqs = decode_keys.shape[0]
    all_rows = jnp.concatenate([piece_tokens, decode_tokens], axis=0)
    normed_in = rms_scaled(all_rows, norm_gain).astype(jnp.bfloat16)
    queries = jnp.dot(normed_in, w_query, preferred_element_type=jnp.float32).astype(jnp.bfloat16)
    new_keys = jnp.dot(normed_in, w_key, preferred_element_type=jnp.float32).astype(jnp.bfloat16)
    new_values = jnp.dot(normed_in, w_value, preferred_element_type=jnp.float32).astype(
        jnp.bfloat16
    )
    normed_out = attend(
        nz, ny, tp, queries[:rows], new_keys[:rows], new_values[:rows], queries[rows:], prompt_keys,
        prompt_values, decode_keys, decode_values, out_gain, score_offset, context_length,
        decoding_cache_length,
    )
    outputs = jnp.dot(normed_out, w_out, preferred_element_type=jnp.float32).astype(jnp.bfloat16)
    return (
        outputs[:rows],
        outputs[rows : rows + seqs],
        new_keys[:rows],
        new_values[:rows],
        new_keys[rows:],
        new_values[rows:],
    )


def solution(mesh):
    in_specs = (
        P("kv", None),
        P("kv", None),
        P(),
        P(None, "tp"),
        P(None, "tp"),
        P(None, "tp"),
        P(),
        P(),
        P("kv", "tp"),
        P("kv", "tp"),
        P("kv", None, "tp"),
        P("kv", None, "tp"),
        P("kv"),
        P(),
        P(None, "tp"),
    )
    out_specs = (
        P("kv", "tp"),
        P("kv", "tp"),
        P("kv", "tp"),
        P("kv", "tp"),
        P("kv", "tp"),
        P("kv", "tp"),
    )
    return jax.shard_map(body, mesh=mesh, in_specs=in_specs, out_specs=out_specs, check_vma=False)
```

time: 106 us -> 86.6 us (0.82)
  Pallas kernels: 84.6 us -> 68.6 us
  local copies, waits for them, and re-layouts: 7.92 us -> 6.46 us
  other arithmetic: 3.63 us -> 2.27 us
    pallas_call x1, Pallas kernels: 84.6 us -> 68.6 us  [attend(): pl.pallas_call(functools.partial(attention_kernel, nz, ny, tp, heads), ou...]
    select_n x2 -> x0, other arithmetic: 1.36 us -> none  [the longest x1 0.68 us: body(): jnp.where(places[None, :] < context_length[0], offset[:, None], HIDDEN)]
where the time goes in v1:
time: 86.6 us; the launch traced here: 86.3 us
  Pallas kernels  68.6 us (79%)
  matrix products  6.99 us (8%)
  local copies, waits for them, and re-layouts  6.46 us (7%)
  other arithmetic  2.27 us (3%)
  between operations  1.99 us (2%)
    pallas_call x1, Pallas kernels, attend(): pl.pallas_call(functools.partial(attention_kernel, nz, ny, tp, heads), ou...  68.6 us
    dot_general x1, matrix products, body(): jnp.dot(normed_in, w_key, preferred_element_type=jnp.float32)  3.46 us
    dot_general x1, matrix products, body(): jnp.dot(normed_out, w_out, preferred_element_type=jnp.float32)  1.85 us

profile of v1, /device:TPU:9, one launch (start us, length us, event | category | flops | bytes accessed | tf_op | source)
XLA Modules:
  0.0 86.3 jit_solution(17134168960087447713)
XLA Ops:
  1.9 1.6 %fusion = f32[129]{0:T(256)S(1)} fusion(bf16[1,4096]{1,0:T(2,128)(2,1)} %param.16, bf16[128,4096]{1,0:T(8,128)(2,1)} %param.15), kind=kLoop, calls=%fused_computation.2 | loop fusion | flops 3170175 | bytes 1057284 | tf_op jit(solution)/shard_map/reduce_sum | solution.py:20
  3.5 1.3 %broadcast_in_dim.2.gain_ref = bf16[1,2048]{1,0:T(2,128)(2,1)} reshape(bf16[2048]{0:T(1024)(128)(2,1)} %param.28) | data formatting | bytes 8192 | tf_op jit(solution)/shard_map/broadcast_in_dim | solution.py:504
  4.8 0.7 convert_element_type.22
  5.5 0.0 copy-start.1
  5.5 0.0 copy-start.2
  5.5 0.0 copy-start.3
  5.5 3.5 %convolution_convert_fusion.2 = bf16[129,512]{1,0:T(8,128)(2,1)S(1)} fusion(bf16[4096,512]{1,0:T(8,128)(2,1)} %param.19, f32[4096]{0:T(1024)S(1)} %convert_element_type.22, f32[129]{0:T(256)S(1)} %add_rsqrt_fusion, bf16[1,4096]{1,0:T(2,128)(2,1)} %param.16, bf16[128,4096]{1,0:T(8,128)(2,1)} %param.15), kind=kOutput, calls=%fused_computation.7 | convolution fusion | flops 544829952 | bytes 5400068 | tf_op jit(solution)/shard_map/dot_general | solution.py:519
  9.0 0.6 slice.40
  9.5 0.7 slice.35.k_ref
  10.2 0.0 copy-done.1
  10.2 0.0 copy-done.2
  10.2 0.0 copy-done.3
  10.2 0.0 copy-start.4
  10.2 0.8 convolution_convert_fusion.1
  11.1 0.6 slice.41
  11.7 0.7 slice.36.v_ref
  12.3 0.1 copy-done.4
  12.4 0.8 convolution_convert_fusion.3
  13.3 0.6 slice.37.dq_ref
  13.8 0.7 slice.34.q_ref
  14.5 0.0 copy-start
  14.5 68.6 %attend.1 = bf16[144,2048]{1,0:T(8,128)(2,1)} custom-call(bf16[128,512]{1,0:T(8,128)(2,1)} %slice.34.q_ref, bf16[128,512]{1,0:T(8,128)(2,1)} %slice.35.k_ref, bf16[128,512]{1,0:T(8,128)(2,1)} %slice.36.v_ref, bf16[1,512]{1,0:T(2,128)(2,1)} %slice.37.dq_ref, bf16[1024,512]{1,0:T(8,128)(2,1)} %ck_ref.1, bf16[1024,512]{1,0:T(8,128)(2,1)} %cv_ref.1, ...), custom_call_target="tpu_custom_call" | custom-call | tf_op jit(solution)/shard_map/attend/pallas_call | solution.py:475
  83.1 0.0 copy-done
  83.1 1.8 %convolution_convert_fusion = bf16[144,1024]{1,0:T(8,128)(2,1)S(1)} fusion(bf16[144,2048]{1,0:T(8,128)(2,1)} %attend.1, bf16[2048,1024]{1,0:T(8,128)(2,1)S(1)} %copy-done), kind=kOutput, calls=%fused_computation.5 | convolution fusion | flops 604127232 | bytes 5079040 | tf_op jit(solution)/shard_map/dot_general | solution.py:528
  84.9 0.6 slice.39
  85.5 0.7 slice.38
  (1 shorter events, 0.0 us)
Async XLA Ops:
  5.5 4.7 %copy-start.1 = (bf16[128,4096]{1,0:T(8,128)(2,1)S(1)}, bf16[128,4096]{1,0:T(8,128)(2,1)}, u32[]{:S(2)}) copy-start(bf16[128,4096]{1,0:T(8,128)(2,1)} %param.15) | copy-start | bytes 3145732
  5.5 4.7 %copy-start.2 = (bf16[1,4096]{1,0:T(2,128)(2,1)S(1)}, bf16[1,4096]{1,0:T(2,128)(2,1)}, u32[]{:S(2)}) copy-start(bf16[1,4096]{1,0:T(2,128)(2,1)} %param.16) | copy-start | bytes 24580
  5.5 4.7 %copy-start.3 = (bf16[4096,512]{1,0:T(8,128)(2,1)S(1)}, bf16[4096,512]{1,0:T(8,128)(2,1)}, u32[]{:S(2)}) copy-start(bf16[4096,512]{1,0:T(8,128)(2,1)} %param.20) | copy-start | bytes 12582916
  10.2 2.2 %copy-start.4 = (bf16[4096,512]{1,0:T(8,128)(2,1)S(1)}, bf16[4096,512]{1,0:T(8,128)(2,1)}, u32[]{:S(2)}) copy-start(bf16[4096,512]{1,0:T(8,128)(2,1)} %param.18) | copy-start | bytes 12582916
  14.5 68.6 %copy-start = (bf16[2048,1024]{1,0:T(8,128)(2,1)S(1)}, bf16[2048,1024]{1,0:T(8,128)(2,1)}, u32[]{:S(2)}) copy-start(bf16[2048,1024]{1,0:T(8,128)(2,1)} %param.29) | copy-start | bytes 12582916

commit v2 on v1

--- a/solution.py
+++ b/solution.py
@@ -18,7 +18,7 @@
 def rms_scaled(rows, gain):
     values = rows.astype(jnp.float32)
     inverse = lax.rsqrt(jnp.mean(values * values, axis=-1, keepdims=True) + EPS)
-    return values * inverse * gain.astype(jnp.float32)
+    return values * inverse * gain
 
 
 def suffix_matrix(size):
@@ -92,22 +92,24 @@
 
 
 def attention_kernel(
-    nz, ny, tp, heads, q_ref, k_ref, v_ref, dq_ref, ck_ref, cv_ref, dk_ref, dv_ref, gain_ref, off_ref,
-    ctx_ref, len_ref, out_ref,
+    nz, ny, tp, heads, x_hbm, d_hbm, wq_hbm, wk_hbm, wv_hbm, ck_hbm, cv_hbm, dk_hbm, dv_hbm, wo_hbm,
+    in_gain_ref, gain_ref, off_ref, ctx_ref, len_ref, out_ref, dec_ref, k_out, v_out, dec_k_ref, dec_v_ref,
+    x_ref, d_ref, wq_ref, wk_ref, wv_ref, ck_ref, cv_ref, dk_ref, dv_ref, wo_ref,
+    xs, q_ref, k_ref, v_ref, dq_ref, normed,
     qg, kp, vt, tab, zbuf, own, obuf, tbuf, oy, ty, mix, zs, zt, zr, ztr, zmix,
     kvb, kvg, qp, pz, pacc, plat, ps, pt, pr, ptr, att, attg,
     q_ys, q_zs, q_fs, q_rs, kv_zs, kv_ys, kv_fs, kv_rs, oy_s, oy_r, ty_s, ty_r, oz_s, oz_r, tz_s, tz_r,
-    p_s, p_r, pt_s, pt_r, a_s, a_r,
+    p_s, p_r, pt_s, pt_r, a_s, a_r, b_s, load_s, w_s, keep_s,
 ):
     n = nz * ny
     me = lax.axis_index("kv")
     mine = lax.axis_index("tp")
     z = me // ny
     y = lax.rem(me, ny)
-    rows = q_ref.shape[0]
+    rows = x_hbm.shape[0]
     width = heads * HEAD
     cache_rows = ck_ref.shape[0]
-    seqs, slots = dk_ref.shape[0], dk_ref.shape[1]
+    seqs, slots = dk_hbm.shape[0], dk_hbm.shape[1]
     scale = HEAD ** (-0.5)
     scale2 = scale * LOG2E
     halves = nz // heads
@@ -134,11 +136,60 @@
     def head_cols(h):
         return pl.ds(h * HEAD, HEAD)
 
+    feed = pltpu.make_async_copy(x_hbm, x_ref, load_s.at[4])
+    feed.start()
+    feed_one = pltpu.make_async_copy(d_hbm, d_ref, load_s.at[5])
+    feed_one.start()
+    pieces_in = w_s.shape[1]
+    depth = x_hbm.shape[1] // pieces_in
+
+    def weight(i, c):
+        src, dst = ((wq_hbm, wq_ref), (wk_hbm, wk_ref), (wv_hbm, wv_ref))[i]
+        at = pl.ds(c * depth, depth)
+        return pltpu.make_async_copy(src.at[at, :], dst.at[at, :], w_s.at[i, c])
+
+    for i in range(3):
+        for c in range(pieces_in):
+            weight(i, c).start()
+    loads = [
+        pltpu.make_async_copy(src, dst, load_s.at[i])
+        for i, (src, dst) in enumerate(
+            ((ck_hbm, ck_ref), (cv_hbm, cv_ref), (dk_hbm, dk_ref), (dv_hbm, dv_ref))
+        )
+    ]
+    for load in loads:
+        load.start()
+    load_out = pltpu.make_async_copy(wo_hbm, wo_ref, load_s.at[6])
+    load_out.start()
+
     barrier = pltpu.get_barrier_semaphore()
     for s in range(1, n):
         pl.semaphore_signal(barrier, inc=1, device_id={"kv": lax.rem(me + s, n)}, device_id_type=MESH)
     for s in range(1, tp):
         pl.semaphore_signal(barrier, inc=1, device_id={"tp": lax.rem(mine + s, tp)}, device_id_type=MESH)
+
+    feed_one.wait()
+    feed.wait()
+    gain_in = in_gain_ref[...].astype(jnp.float32)[None, :]
+    xs[pl.ds(0, rows), :] = rms_scaled(x_ref[...], gain_in).astype(jnp.bfloat16)
+    line = lax.broadcasted_iota(jnp.int32, (16, x_ref.shape[1]), 0)
+    single = jnp.zeros((16, x_ref.shape[1]), jnp.float32)
+    for b in range(seqs):
+        single = jnp.where(line == b, rms_scaled(d_ref[b : b + 1, :], gain_in), single)
+    xs[pl.ds(rows, 16), :] = single.astype(jnp.bfloat16)
+
+    def projected(i):
+        total = None
+        for c in range(pieces_in):
+            weight(i, c).wait()
+            at = pl.ds(c * depth, depth)
+            part = dot(xs[:, at], (wq_ref, wk_ref, wv_ref)[i][at, :])
+            total = part if total is None else total + part
+        return total.astype(jnp.bfloat16)
+
+    projection = projected(0)
+    q_ref[...] = projection[0:rows]
+    dq_ref[...] = projection[rows:]
     pl.semaphore_wait(barrier, n - 1 + tp - 1)
 
     def remote(src, dst, ss, rs, peer, axis="kv"):
@@ -162,6 +213,18 @@
         q_column(k).start()
     qg[me] = q_ref[...]
 
+    projection = projected(1)
+    k_ref[...] = projection[0:rows]
+    dec_k_ref[...] = projection[rows : rows + seqs]
+    projection = projected(2)
+    v_ref[...] = projection[0:rows]
+    dec_v_ref[...] = projection[rows : rows + seqs]
+    keeps = [
+        pltpu.make_async_copy(k_ref, k_out, keep_s.at[0]),
+        pltpu.make_async_copy(v_ref, v_out, keep_s.at[1]),
+    ]
+    for keep in keeps:
+        keep.start()
     short = spread_matrix(rows)
     for h in range(heads):
         kvb[h, 0:rows, :] = dot(short, k_ref[:, head_cols(h)]).astype(jnp.bfloat16)
@@ -182,6 +245,8 @@
         kv_column(k).start()
     kvg[me] = kvb[my_head]
 
+    loads[0].wait()
+    loads[1].wait()
     run = cache_rows // 8
     tiles = run // 32
     wide = spread_matrix(256)
@@ -200,6 +265,8 @@
     for h in range(heads):
         tab[h] = jnp.where(valid, off_ref[mine * heads + h] * LOG2E, HIDDEN)
 
+    loads[2].wait()
+    loads[3].wait()
     chunk = 256 if slots % 256 == 0 else 128
     suffix = suffix_matrix(chunk)
     hrow = lax.broadcasted_iota(jnp.int32, (8, width), 0)
@@ -225,13 +292,11 @@
         dec_rows = jnp.where(place == b, line, dec_rows)
     att[pl.ds(rows, 16), :] = dec_rows.astype(att.dtype)
 
-    def forward(s):
+    def forward(block, s):
         c = source(s) * ny + y
-        q_block(c, s, 0).wait_recv()
-        kv_block(c, s, 0).wait_recv()
+        block(c, s, 0).wait_recv()
         for k in range(1, ny):
-            q_block(c, s, k).start()
-            kv_block(c, s, k).start()
+            block(c, s, k).start()
 
     def piece_out(j):
         return remote(ps.at[j], pr.at[my_head], p_s.at[j], p_r.at[my_head], (my_part + halves * j) * ny + y)
@@ -370,10 +435,15 @@
 
     def step(s, carry):
         u = source(s)
-        pl.when(s + 1 < nz)(lambda: forward(s + 1))
+        pl.when(s + 1 < nz)(lambda: forward(q_block, s + 1))
+
+        @pl.when(s == nz - 1)
+        def _():
+            for r in range(1, nz):
+                forward(kv_block, r)
+
         for k in range(1, ny):
             q_block(u * ny + other(k), 0, 0).wait_recv()
-        pl.when(s == nz - 1)(pieces)
         compute(u)
         for k in range(1, ny):
             o_column(u, s, k).start()
@@ -382,6 +452,7 @@
         return carry
 
     lax.fori_loop(0, nz, step, 0)
+    pieces()
     combine(nz - 1)
 
     for h in range(heads):
@@ -410,10 +481,19 @@
         total = total * ptr[h, 0:1, :] + pr[h].astype(jnp.float32)
         att[pl.ds(0, rows), head_cols(h)] = jnp.transpose(total).astype(att.dtype)
 
-    for s in range(1, tp):
-        peer = lax.rem(mine + s, tp)
-        remote(att, attg.at[mine], a_s.at[s], a_r.at[mine], peer, "tp").start()
+    core = lax.rem(mine, 2)
+    sibling = mine + 1 - 2 * core
+
+    def across(s):
+        return remote(att, attg.at[mine], a_s.at[s], a_r.at[mine], lax.rem(mine + 2 * s, tp), "tp")
+
+    def beside(c):
+        return remote(attg.at[c], attg.at[c], b_s.at[c], a_r.at[c], sibling, "tp")
+
+    for s in range(1, tp // 2):
+        across(s).start()
     attg[mine] = att[...]
+    remote(att, attg.at[mine], a_s.at[0], a_r.at[mine], sibling, "tp").start()
 
     for s in range(1, nz):
         q_plane(s).wait_send()
@@ -439,31 +519,63 @@
             piece_out(j).wait_send()
             piece_total(j).wait_send()
 
-    for s in range(1, tp):
-        peer = lax.rem(mine + s, tp)
-        remote(att, attg.at[peer], a_s.at[s], a_r.at[peer], peer, "tp").wait()
+    for s in range(1, tp // 2):
+        c = lax.rem(mine + tp - 2 * s, tp)
+        beside(c).wait_recv()
+        beside(c).start()
+    for s in range(tp // 2):
+        beside(lax.rem(sibling + 2 * s, tp)).wait_recv()
+    remote(att, attg.at[mine], a_s.at[0], a_r.at[mine], sibling, "tp").wait_send()
+    for s in range(1, tp // 2):
+        across(s).wait_send()
+        beside(lax.rem(mine + tp - 2 * s, tp)).wait_send()
     square = jnp.zeros((att.shape[0], 1), jnp.float32)
     for t in range(tp):
         values = attg[t].astype(jnp.float32)
         square += jnp.sum(values * values, axis=-1, keepdims=True)
     inverse = lax.rsqrt(square / (tp * width) + EPS)
+    gain_out = gain_ref[...].astype(jnp.float32)[None, :]
     for t in range(tp):
-        cols = pl.ds(t * width, width)
-        gain = gain_ref[0:1, cols].astype(jnp.float32)
-        out_ref[:, cols] = (attg[t].astype(jnp.float32) * inverse * gain).astype(out_ref.dtype)
-
-
-def attend(
-    nz, ny, tp, queries, keys, values, decode_queries, prompt_keys, prompt_values, decode_keys, decode_values,
-    out_gain, score_offset, context_length, decoding_cache_length,
+        cols = slice(t * width, t * width + width)
+        normed[:, cols] = (attg[t].astype(jnp.float32) * inverse * gain_out[:, cols]).astype(jnp.bfloat16)
+    load_out.wait()
+    result = dot(normed[...], wo_ref[...]).astype(jnp.bfloat16)
+    out_ref[...] = result[0:rows]
+    dec_ref[...] = result[rows : rows + seqs]
+    for keep in keeps:
+        keep.wait()
+
+
+def deliver_kernel(*refs):
+    sems = refs[-1]
+    count = sems.shape[1]
+    sources, targets, held = refs[:count], refs[count : 2 * count], refs[2 * count : 3 * count]
+    taken = [pltpu.make_async_copy(sources[i], held[i], sems.at[0, i]) for i in range(count)]
+    given = [pltpu.make_async_copy(held[i], targets[i], sems.at[1, i]) for i in range(count)]
+    for i in range(count):
+        taken[i].start()
+    for i in range(count):
+        taken[i].wait()
+        given[i].start()
+    for i in range(count):
+        given[i].wait()
+
+
+def body(
+    piece_tokens, decode_tokens, norm_gain, w_query, w_key, w_value, score_offset, context_length,
+    prompt_keys, prompt_values, decode_keys, decode_values, decoding_cache_length, out_gain, w_out,
 ):
-    n = nz * ny
-    rows, width = queries.shape
+    n, tp = lax.axis_size("kv"), lax.axis_size("tp")
+    nz, ny = grid_of(n)
+    rows, model = piece_tokens.shape
+    width = w_query.shape[1]
+    seqs = decode_keys.shape[0]
     heads = width // HEAD
-    assert nz % heads == 0
+    assert nz % heads == 0 and tp % 2 == 0
     cache_rows = prompt_keys.shape[0]
     vmem = pl.BlockSpec(memory_space=pltpu.VMEM)
     smem = pl.BlockSpec(memory_space=pltpu.SMEM)
+    hbm = pl.BlockSpec(memory_space=pl.ANY)
     dma = pltpu.SemaphoreType.DMA
 
     def half(*shape):
@@ -472,12 +584,23 @@
     def full(*shape):
         return pltpu.VMEM(shape, jnp.float32)
 
-    return pl.pallas_call(
+    def result(*shape):
+        return jax.ShapeDtypeStruct(shape, jnp.bfloat16)
+
+    results = pl.pallas_call(
         functools.partial(attention_kernel, nz, ny, tp, heads),
-        out_shape=jax.ShapeDtypeStruct((rows + 16, tp * width), jnp.bfloat16),
-        in_specs=[vmem] * 9 + [smem] * 3,
-        out_specs=vmem,
+        out_shape=(
+            result(rows, w_out.shape[1]), result(seqs, w_out.shape[1]), result(rows, width), result(rows, width),
+            result(seqs, width), result(seqs, width),
+        ),
+        in_specs=[hbm] * 10 + [vmem] * 2 + [smem] * 3,
+        out_specs=(vmem, vmem, hbm, hbm, vmem, vmem),
         scratch_shapes=[
+            half(rows, model), half(seqs, model), half(model, width), half(model, width), half(model, width),
+            half(*prompt_keys.shape), half(*prompt_values.shape), half(*decode_keys.shape), half(*decode_values.shape),
+            half(*w_out.shape),
+            half(rows + 16, model), half(rows, width), half(rows, width), half(rows, width), half(16, width),
+            half(rows + 16, tp * width),
             half(n, rows, width), half(heads, cache_rows, HEAD), half(heads, HEAD, cache_rows),
             full(heads, cache_rows, 128), full(heads, cache_rows, ny * rows),
             full(nz, ny, width, rows), half(nz, ny, width, rows), full(nz, ny, 8, 128),
@@ -493,47 +616,25 @@
             dma((nz, ny)), dma((nz, ny)), dma((nz, ny)), dma((nz, ny)),
             dma((nz,)), dma((nz,)), dma((nz,)), dma((nz,)),
             dma((heads,)), dma((heads,)), dma((heads,)), dma((heads,)),
-            dma((tp,)), dma((tp,)),
+            dma((tp,)), dma((tp,)), dma((tp,)), dma((7,)), dma((3, 8)), dma((2,)),
         ],
         compiler_params=pltpu.CompilerParams(
-            collective_id=0, has_side_effects=True, vmem_limit_bytes=56 * 1024 * 1024
+            collective_id=0, has_side_effects=True, vmem_limit_bytes=60 * 1024 * 1024
         ),
         name="attend",
     )(
-        queries, keys, values, decode_queries, prompt_keys, prompt_values, decode_keys, decode_values,
-        out_gain[None, :], score_offset, context_length, decoding_cache_length,
+        piece_tokens, decode_tokens, w_query, w_key, w_value, prompt_keys, prompt_values, decode_keys, decode_values,
+        w_out, norm_gain, out_gain, score_offset, context_length, decoding_cache_length,
     )
-
-
-def body(
-    piece_tokens, decode_tokens, norm_gain, w_query, w_key, w_value, score_offset, context_length,
-    prompt_keys, prompt_values, decode_keys, decode_values, decoding_cache_length, out_gain, w_out,
-):
-    n, tp = lax.axis_size("kv"), lax.axis_size("tp")
-    nz, ny = grid_of(n)
-    rows = piece_tokens.shape[0]
-    seqs = decode_keys.shape[0]
-    all_rows = jnp.concatenate([piece_tokens, decode_tokens], axis=0)
-    normed_in = rms_scaled(all_rows, norm_gain).astype(jnp.bfloat16)
-    queries = jnp.dot(normed_in, w_query, preferred_element_type=jnp.float32).astype(jnp.bfloat16)
-    new_keys = jnp.dot(normed_in, w_key, preferred_element_type=jnp.float32).astype(jnp.bfloat16)
-    new_values = jnp.dot(normed_in, w_value, preferred_element_type=jnp.float32).astype(
-        jnp.bfloat16
-    )
-    normed_out = attend(
-        nz, ny, tp, queries[:rows], new_keys[:rows], new_values[:rows], queries[rows:], prompt_keys,
-        prompt_values, decode_keys, decode_values, out_gain, score_offset, context_length,
-        decoding_cache_length,
-    )
-    outputs = jnp.dot(normed_out, w_out, preferred_element_type=jnp.float32).astype(jnp.bfloat16)
-    return (
-        outputs[:rows],
-        outputs[rows : rows + seqs],
-        new_keys[:rows],
-        new_values[:rows],
-        new_keys[rows:],
-        new_values[rows:],
-    )
+    kinds = [jax.ShapeDtypeStruct(r.shape, r.dtype) for r in results]
+    return pl.pallas_call(
+        deliver_kernel,
+        out_shape=kinds,
+        in_specs=[hbm] * len(kinds),
+        out_specs=[hbm] * len(kinds),
+        scratch_shapes=[pltpu.VMEM(k.shape, k.dtype) for k in kinds] + [dma((2, len(kinds)))],
+        name="deliver",
+    )(*results)
 
 
 def solution(mesh):

time: 86.6 us -> 64.1 us (0.74)
  Pallas kernels: 68.6 us -> 61.4 us
  matrix products: 6.99 us -> 0 us
  local copies, waits for them, and re-layouts: 6.46 us -> 0 us
  other arithmetic: 2.27 us -> 0 us
    pallas_call x1 -> x2, Pallas kernels: 68.6 us -> 61.4 us  [the longest x1 59.6 us: body(): pl.pallas_call(functools.partial(attention_kernel, nz, ny, tp, heads), ou...]
    dot_general x4 -> x0, matrix products: 6.99 us -> none  [the longest x1 3.46 us: body(): jnp.dot(normed_in, w_key, preferred_element_type=jnp.float32)]
    slice x8 -> x0, local copies, waits for them, and re-layouts: 5.06 us -> none  [the longest x1 0.72 us: body(): outputs[:rows]]
    reduce_sum x1 -> x0, other arithmetic: 1.56 us -> none  [rms_scaled(): inverse = lax.rsqrt(jnp.mean(values * values, axis=-1, keepdims=True) + EPS)]
    broadcast_in_dim x1 -> x0, local copies, waits for them, and re-layouts: 1.29 us -> none  [attend(): out_gain[None, :]]
where the time goes in v2:
time: 64.1 us; the launch traced here: 63.4 us
  Pallas kernels  61.4 us (96%)
  between operations  1.94 us (3%)
    pallas_call x1, Pallas kernels, body(): pl.pallas_call(functools.partial(attention_kernel, nz, ny, tp, heads), ou...  59.6 us
    pallas_call x1, Pallas kernels, body(): pl.pallas_call(deliver_kernel, out_shape=kinds, in_specs=[hbm] * len(kind...  1.85 us

profile of v2, /device:TPU:9, one launch (start us, length us, event | category | flops | bytes accessed | tf_op | source)
XLA Modules:
  0.0 63.4 jit_solution(10943827567949936285)
XLA Ops:
  1.9 59.6 %attend.1 = (bf16[128,1024]{1,0:T(8,128)(2,1)}, bf16[1,1024]{1,0:T(2,128)(2,1)}, bf16[128,512]{1,0:T(8,128)(2,1)}, bf16[128,512]{1,0:T(8,128)(2,1)}, bf16[1,512]{1,0:T(2,128)(2,1)}, /*index=5*/bf16[1,512]{1,0:T(2,128)(2,1)}) custom-call(bf16[128,4096]{1,0:T(8,128)(2,1)} %x_hbm.1, bf16[1,4096]{1,0:T(2,128)(2,1)} %d_hbm.1, bf16[4096,512]{1,0:T(8,128)(2,1)} %wq_hbm.1, ...), custom_call_target="tpu_custom_call" | custom-call | tf_op jit(solution)/shard_map/attend/pallas_call | solution.py:590
  61.5 1.8 %deliver.1 = (bf16[128,1024]{1,0:T(8,128)(2,1)}, bf16[1,1024]{1,0:T(2,128)(2,1)}, bf16[128,512]{1,0:T(8,128)(2,1)}, bf16[128,512]{1,0:T(8,128)(2,1)}, bf16[1,512]{1,0:T(2,128)(2,1)}, /*index=5*/bf16[1,512]{1,0:T(2,128)(2,1)}) custom-call(bf16[128,1024]{1,0:T(8,128)(2,1)} %get-tuple-element.12.refs_0_, bf16[1,1024]{1,0:T(2,128)(2,1)} %get-tuple-element.13.refs_1_, ...), custom_call_target="tpu_custom_call" | custom-call | tf_op jit(solution)/shard_map/deliver/pallas_call | solution.py:630

commit v3 on v2

v3 whole, which is shorter than its diff:
```python
import functools
import math

import jax
import jax.numpy as jnp
from jax import lax
from jax.experimental import pallas as pl
from jax.experimental.pallas import tpu as pltpu
from jax.sharding import PartitionSpec as P

HEAD = 128
EPS = 1e-06
HIDDEN = -1e30
LAG = 3
KV_AT = 2
LOG2E = 1.4426950408889634
MESH = pl.DeviceIdType.MESH


def rms_scaled(rows, gain):
    values = rows.astype(jnp.float32)
    inverse = lax.rsqrt(jnp.mean(values * values, axis=-1, keepdims=True) + EPS)
    return values * inverse * gain


def suffix_matrix(size):
    row = lax.broadcasted_iota(jnp.int32, (size, size), 0)
    column = lax.broadcasted_iota(jnp.int32, (size, size), 1)
    return jnp.where(row >= column, 1.0, 0.0).astype(jnp.bfloat16)


def spread_matrix(size):
    run = size // 8
    row = lax.broadcasted_iota(jnp.int32, (size, size), 0)
    column = lax.broadcasted_iota(jnp.int32, (size, size), 1)
    hit = (row // 8 == column % run) & (row % 8 == column // run)
    return jnp.where(hit, 1.0, 0.0).astype(jnp.bfloat16)


def dot_t(a, b):
    return lax.dot_general(a, b, (((1,), (1,)), ((), ())), preferred_element_type=jnp.float32)


def dot(a, b):
    return jnp.dot(a, b, preferred_element_type=jnp.float32)


def suffix_keep(z, suffix):
    keep = -(jnp.maximum(z, 0.0) + jnp.log(1.0 + jnp.exp(-jnp.abs(z))))
    high = keep.astype(jnp.bfloat16)
    low = (keep - high.astype(jnp.float32)).astype(jnp.bfloat16)
    return dot(high, suffix) + dot(low, suffix)


def cached_terms(query, key_of, value_of, bias_of, total_keys, chunk, suffix, scale):
    later = None
    out = None
    for start in reversed(range(0, total_keys, chunk)):
        z = dot_t(query, key_of(start)) * scale + bias_of(start)
        inner = suffix_keep(z, suffix)
        exponent = z + inner if later is None else z + inner + later
        weight = jnp.exp(exponent).astype(jnp.bfloat16)
        part = dot(weight, value_of(start))
        out = part if out is None else out + part
        later = inner[:, 0:1] if later is None else later + inner[:, 0:1]
    return out, later


def grid_of(n):
    columns = max(d for d in range(1, math.isqrt(n) + 1) if n % d == 0)
    return n // columns, columns


def later_sublanes(runs):
    place = lax.broadcasted_iota(jnp.int32, runs.shape, 0)

    def up(x, k):
        return jnp.where(place < 8 - k, pltpu.roll(x, 8 - k, 0), 1.0)

    x = up(runs, 1)
    x = x * up(x, 1)
    x = x * up(x, 2)
    return x * up(x, 4)


def break_sticks(score, store, steps, groups):
    left = [jnp.ones((8, 128), jnp.float32) for _ in range(groups)]
    for v in reversed(range(steps)):
        for g in range(groups):
            e = jnp.exp2(jnp.minimum(score(v, g), 126.0))
            left[g] = left[g] * (1.0 / (1.0 + e))
            store(v, g, e * left[g])
    return left


def attention_kernel(
    nz, ny, tp, heads, parts, x_hbm, d_hbm, wq_hbm, wk_hbm, wv_hbm, ck_hbm, cv_hbm, dk_hbm, dv_hbm, wo_hbm,
    in_gain_ref, gain_ref, off_ref, ctx_ref, len_ref, out_ref, dec_ref, k_out, v_out, dec_k_ref, dec_v_ref,
    x_ref, d_ref, wq_ref, wk_ref, wv_ref, ck_ref, cv_ref, dk_ref, dv_ref, wo_ref,
    xs, q_ref, k_ref, v_ref, dq_ref, normed,
    qg, kp, vt, tab, zbuf, own, obuf, tbuf, oy, ty, mix, pair, zs, zt, zr, ztr, zmix, zmine,
    kvb, kvg, qp, pz, pout, pacc, plat, ps, pt, pr, ptr, att, attg,
    q_ys, q_zs, q_fs, q_rs, kv_zs, kv_ys, kv_fs, kv_rs, oy_s, oy_r, ty_s, ty_r, oz_s, oz_r, tz_s, tz_r,
    p_s, p_r, pt_s, pt_r, a_s, a_r, b_s, load_s, w_s, keep_s, q_hs,
):
    n = nz * ny
    me = lax.axis_index("kv")
    mine = lax.axis_index("tp")
    z = me // ny
    y = lax.rem(me, ny)
    rows = x_hbm.shape[0]
    width = heads * HEAD
    share = heads // parts
    band = share * HEAD
    cache_rows = ck_ref.shape[0]
    seqs, slots = dk_hbm.shape[0], dk_hbm.shape[1]
    scale = HEAD ** (-0.5)
    scale2 = scale * LOG2E
    halves = nz // heads
    my_head = lax.rem(z, heads)
    my_part = z // heads
    bits = nz.bit_length() - 1
    far = nz == 4

    def source(s):
        total = 0
        for b in range(bits):
            total += lax.rem(lax.rem(z // (1 << b), 2) + lax.rem(s // (1 << b), 2), 2) * (1 << b)
        return total

    def other(k):
        return lax.rem(y + k, ny)

    def head_cols(h):
        return pl.ds(h * HEAD, HEAD)

    feed = pltpu.make_async_copy(x_hbm, x_ref, load_s.at[4])
    feed.start()
    feed_one = pltpu.make_async_copy(d_hbm, d_ref, load_s.at[5])
    feed_one.start()
    pieces_in = w_s.shape[1]
    depth = x_hbm.shape[1] // pieces_in

    def weight(i, c):
        src, dst = ((wq_hbm, wq_ref), (wk_hbm, wk_ref), (wv_hbm, wv_ref))[i]
        at = pl.ds(c * depth, depth)
        return pltpu.make_async_copy(src.at[at, :], dst.at[at, :], w_s.at[i, c])

    for c in range(pieces_in):
        weight(0, c).start()
    loads = [
        pltpu.make_async_copy(src, dst, load_s.at[i])
        for i, (src, dst) in enumerate(
            ((ck_hbm, ck_ref), (cv_hbm, cv_ref), (dk_hbm, dk_ref), (dv_hbm, dv_ref))
        )
    ]
    loads[0].start()
    loads[1].start()
    for i in range(1, 3):
        for c in range(pieces_in):
            weight(i, c).start()
    loads[2].start()
    loads[3].start()
    load_out = pltpu.make_async_copy(wo_hbm, wo_ref, load_s.at[6])
    load_out.start()

    barrier = pltpu.get_barrier_semaphore()
    for s in range(1, n):
        pl.semaphore_signal(barrier, inc=1, device_id={"kv": lax.rem(me + s, n)}, device_id_type=MESH)
    for s in range(1, tp):
        pl.semaphore_signal(barrier, inc=1, device_id={"tp": lax.rem(mine + s, tp)}, device_id_type=MESH)

    feed_one.wait()
    feed.wait()
    gain_in = in_gain_ref[...].astype(jnp.float32)[None, :]
    xs[pl.ds(0, rows), :] = rms_scaled(x_ref[...], gain_in).astype(jnp.bfloat16)
    line = lax.broadcasted_iota(jnp.int32, (16, x_ref.shape[1]), 0)
    single = jnp.zeros((16, x_ref.shape[1]), jnp.float32)
    for b in range(seqs):
        single = jnp.where(line == b, rms_scaled(d_ref[b : b + 1, :], gain_in), single)
    xs[pl.ds(rows, 16), :] = single.astype(jnp.bfloat16)

    def projected(i):
        total = None
        for c in range(pieces_in):
            weight(i, c).wait()
            at = pl.ds(c * depth, depth)
            part = dot(xs[:, at], (wq_ref, wk_ref, wv_ref)[i][at, :])
            total = part if total is None else total + part
        return total.astype(jnp.bfloat16)

    projection = projected(0)
    for p in range(parts):
        q_ref[p] = projection[0:rows, p * band : p * band + band]
    dq_ref[...] = projection[rows:]
    pl.semaphore_wait(barrier, n - 1 + tp - 1)

    def remote(src, dst, ss, rs, peer, axis="kv"):
        return pltpu.make_async_remote_copy(
            src_ref=src, dst_ref=dst, send_sem=ss, recv_sem=rs,
            device_id={axis: peer}, device_id_type=MESH,
        )

    def q_plane(s, p):
        return remote(q_ref.at[p], qg.at[me, p], q_zs.at[s, p], q_rs.at[me, p], source(s) * ny + y)

    def q_column(k, p):
        return remote(q_ref.at[p], qg.at[me, p], q_ys.at[k, p], q_rs.at[me, p], z * ny + other(k))

    def q_block(c, s, p, k):
        return remote(qg.at[c, p], qg.at[c, p], q_fs.at[s, p, k], q_rs.at[c, p], z * ny + other(k))

    def q_relay(s, p):
        c = source(s) * ny + y
        return remote(qg.at[c, p], qg.at[c, p], q_hs.at[p], q_rs.at[c, p], source(1) * ny + y)

    direct = (2, 1) if far else (1,)
    for s in direct:
        for p in range(parts):
            q_plane(s, p).start()
    for k in range(1, ny):
        for p in range(parts):
            q_column(k, p).start()
    qg[me] = q_ref[...]

    loads[0].wait()
    loads[1].wait()
    run = cache_rows // 8
    tiles = run // 32
    wide = spread_matrix(256)
    for t in range(tiles):
        def strip(ref):
            return jnp.concatenate([ref[pl.ds(s * run + t * 32, 32), :] for s in range(8)], axis=0)
        keys = dot(wide, strip(ck_ref)).astype(jnp.bfloat16)
        values = dot(wide, strip(cv_ref))
        for h in range(heads):
            kp[h, t * 256 : t * 256 + 256, :] = keys[:, h * HEAD : h * HEAD + HEAD]
            vt[h, :, t * 256 : t * 256 + 256] = jnp.transpose(
                values[:, h * HEAD : h * HEAD + HEAD]
            ).astype(jnp.bfloat16)
    row = lax.broadcasted_iota(jnp.int32, (cache_rows, 128), 0)
    valid = me * cache_rows + lax.rem(row, 8) * run + row // 8 < ctx_ref[0]
    for h in range(heads):
        tab[h] = jnp.where(valid, off_ref[mine * heads + h] * LOG2E, HIDDEN)

    def forward_q(s, p):
        c = source(s) * ny + y
        q_block(c, s, p, 0).wait_recv()
        if far and s == 2:
            q_relay(s, p).start()
        for k in range(1, ny):
            q_block(c, s, p, k).start()

    def forward_kv(s):
        c = source(s) * ny + y
        kv_block(c, s, 0).wait_recv()
        for k in range(1, ny):
            kv_block(c, s, k).start()

    def piece_out(j):
        return remote(ps.at[j], pr.at[my_head], p_s.at[j], p_r.at[my_head], (my_part + halves * j) * ny + y)

    def piece_total(j):
        return remote(pt.at[j], ptr.at[my_head], pt_s.at[j], pt_r.at[my_head], (my_part + halves * j) * ny + y)

    def pieces():
        for k in range(1, ny):
            for u in range(nz):
                kv_block(u * ny + other(k), 0, 0).wait_recv()
        cols = pl.ds(pl.multiple_of(lax.rem(my_head, share) * HEAD, HEAD), HEAD)
        for j in range(heads):
            qp[j * rows : j * rows + rows, :] = qg[(my_part + halves * j) * ny + y, my_head // share, :, cols]
        pacc[...] = jnp.zeros_like(pacc)
        plat[...] = jnp.ones_like(plat)
        lane = lax.broadcasted_iota(jnp.int32, (8, 128), 1)
        first = lax.broadcasted_iota(jnp.int32, (8, 128), 0) * (rows // 8)
        off = off_ref[mine * heads + my_head] * LOG2E

        batch = 4 if n % 4 == 0 else 1

        def block(c, slot):
            pz[slot] = dot_t(kvg[c, 0:rows, :], qp[...])

            def score(v, g):
                seen = c * rows + first + v < ((my_part + halves * g) * ny + y) * rows + lane
                at = pz[slot, v * 8 : v * 8 + 8, g * 128 : g * 128 + 128]
                return jnp.where(seen, at * scale2 + off, HIDDEN)

            def store(v, g, w):
                pz[slot, v * 8 : v * 8 + 8, g * 128 : g * 128 + 128] = w

            left = break_sticks(score, store, rows // 8, heads)
            factors = [later_sublanes(x) for x in left]
            factor = jnp.concatenate(factors, axis=1)
            w = pz[slot].reshape(rows // 8, 8, heads * rows) * factor[None]
            w = w.reshape(rows, heads * rows).astype(jnp.bfloat16)
            pout[slot] = dot(kvg[c, rows : 2 * rows, :], w)
            return (factor * jnp.concatenate(left, axis=1))[0:1, :]

        def several(i, carry):
            wholes = [block(n - 1 - i * batch - slot, slot) for slot in range(batch)]
            later = plat[0:1, :]
            total = pacc[...]
            for slot in range(batch):
                total += pout[slot] * later
                later = later * wholes[slot]
            pacc[...] = total
            plat[...] = jnp.broadcast_to(later, plat.shape)
            return carry

        lax.fori_loop(0, n // batch, several, 0)
        for j in range(heads):
            owner = my_part + halves * j
            ps[j] = pacc[:, j * rows : j * rows + rows].astype(jnp.bfloat16)
            pt[j] = plat[:, j * rows : j * rows + rows]

            @pl.when(owner != z)
            def _():
                piece_out(j).start()
                piece_total(j).start()

            @pl.when(owner == z)
            def _():
                pr[my_head] = ps[j]
                ptr[my_head] = pt[j]

    def o_column(u, s, p, k):
        return remote(
            obuf.at[u, p, other(k)], oy.at[u, p, y], oy_s.at[s, p, k], oy_r.at[u, p, y], z * ny + other(k)
        )

    def t_column(u, s, p, k):
        return remote(
            tbuf.at[u, p, other(k)], ty.at[u, p, y], ty_s.at[s, p, k], ty_r.at[u, p, y], z * ny + other(k)
        )

    def o_from(u, p, c):
        return remote(obuf.at[u, p, c], oy.at[u, p, c], oy_s.at[0, p, 0], oy_r.at[u, p, c], z * ny + other(1))

    def t_from(u, p, c):
        return remote(tbuf.at[u, p, c], ty.at[u, p, c], ty_s.at[0, p, 0], ty_r.at[u, p, c], z * ny + other(1))

    def compute(u, p):
        totals = [jnp.ones((8, 128), jnp.float32) for _ in range(ny)]
        place = lax.broadcasted_iota(jnp.int32, (8, 128), 0)
        for h in range(share):
            head = p * share + h
            q = qg[pl.ds(u * ny, ny), p, :, head_cols(h)].reshape(ny * rows, HEAD)
            zbuf[h] = dot_t(kp[head], q)

            def score(v, g):
                at = slice(v * 8, v * 8 + 8)
                return zbuf[h, at, g * 128 : g * 128 + 128] * scale2 + tab[head, at, :]

            def store(v, g, w):
                zbuf[h, v * 8 : v * 8 + 8, g * 128 : g * 128 + 128] = w

            left = break_sticks(score, store, run, ny)
            factors = [later_sublanes(x) for x in left]
            factor = jnp.concatenate(factors, axis=1)
            w = zbuf[h].reshape(run, 8, ny * rows) * factor[None]
            out = dot(vt[head], w.reshape(cache_rows, ny * rows).astype(jnp.bfloat16))
            for g in range(ny):
                block = out[:, g * rows : g * rows + rows]
                own[u, p, g, head_cols(h), :] = block
                obuf[u, p, g, head_cols(h), :] = block.astype(jnp.bfloat16)
                totals[g] = jnp.where(place == h, (factors[g] * left[g])[0:1, :], totals[g])
        for g in range(ny):
            tbuf[u, p, g] = totals[g]
        ty[u, p, y] = tbuf[u, p, y]

    def o_plane(s, p):
        return remote(zs.at[s, p], zr.at[s - 1, p], oz_s.at[s, p], oz_r.at[s - 1, p], source(s) * ny + y)

    def t_plane(s, p):
        return remote(zt.at[s, p], ztr.at[s - 1, p], tz_s.at[s, p], tz_r.at[s - 1, p], source(s) * ny + y)

    even = lax.rem(z, 2) == 0
    one = jnp.ones((8, 128), jnp.float32)

    def combine(s, p):
        u = source(s)
        mix[y] = own[u, p, y]
        for k in range(1, ny):
            o_from(u, p, other(k)).wait_recv()
            t_from(u, p, other(k)).wait_recv()
            mix[other(k)] = oy[u, p, other(k)].astype(jnp.float32)
        later = one
        factors = []
        for c in reversed(range(ny)):
            factors.append(later)
            later = later * ty[u, p, c]
        for h in range(share):
            total = jnp.zeros((HEAD, rows), jnp.float32)
            for c in range(ny):
                total += mix[c, head_cols(h), :] * factors[ny - 1 - c][h : h + 1, :]
            pair[head_cols(h), :] = total

        @pl.when(s == 0)
        def _():
            zmix[p] = pair[...]
            zmine[p] = later

        @pl.when(s > 0)
        def _():
            zs[s, p] = pair[...].astype(jnp.bfloat16)
            zt[s, p] = later
            o_plane(s, p).start()
            t_plane(s, p).start()

    def unit(s, p):
        u = source(s)
        for k in range(1, ny):
            q_block(u * ny + other(k), 0, p, 0).wait_recv()
        compute(u, p)
        for k in range(1, ny):
            o_column(u, s, p, k).start()
            t_column(u, s, p, k).start()

    def place_of(t):
        i = t // parts
        turn = lax.rem(lax.rem(i, 2) + i // 2, 2) * 2 + i // 2 if far else i
        return turn, lax.rem(t, parts)

    def step(t, carry):
        unit(*place_of(t))
        pl.when(t >= LAG)(lambda: combine(*place_of(t - LAG)))
        return carry

    def first(t, carry):
        unit(0, t)
        if far:
            forward_q(2, t)
        return carry

    projection = projected(1)
    k_ref[...] = projection[0:rows]
    dec_k_ref[...] = projection[rows : rows + seqs]
    projection = projected(2)
    v_ref[...] = projection[0:rows]
    dec_v_ref[...] = projection[rows : rows + seqs]
    keeps = [
        pltpu.make_async_copy(k_ref, k_out, keep_s.at[0]),
        pltpu.make_async_copy(v_ref, v_out, keep_s.at[1]),
    ]
    for keep in keeps:
        keep.start()
    short = spread_matrix(rows)
    for h in range(heads):
        kvb[h, 0:rows, :] = dot(short, k_ref[:, head_cols(h)]).astype(jnp.bfloat16)
        kvb[h, rows : 2 * rows, :] = jnp.transpose(dot(short, v_ref[:, head_cols(h)])).astype(jnp.bfloat16)

    def kv_plane(t):
        return remote(kvb.at[t % heads], kvg.at[me], kv_zs.at[t], kv_rs.at[me], t * ny + y)

    def kv_column(k):
        return remote(kvb.at[my_head], kvg.at[me], kv_ys.at[k], kv_rs.at[me], z * ny + other(k))

    def kv_block(c, s, k):
        return remote(kvg.at[c], kvg.at[c], kv_fs.at[s, k], kv_rs.at[c], z * ny + other(k))

    for t in range(nz):
        pl.when(z != t)(lambda t=t: kv_plane(t).start())
    for k in range(1, ny):
        kv_column(k).start()
    kvg[me] = kvb[my_head]

    lax.fori_loop(0, parts, first, 0)
    for p in range(parts):
        forward_q(1, p)
    loads[2].wait()
    loads[3].wait()
    chunk = 256 if slots % 256 == 0 else 128
    suffix = suffix_matrix(chunk)
    hrow = lax.broadcasted_iota(jnp.int32, (8, width), 0)
    hcol = lax.broadcasted_iota(jnp.int32, (8, width), 1) // HEAD
    own_head = hrow == hcol
    head_row = lax.broadcasted_iota(jnp.int32, (8, chunk), 0)
    spot = lax.broadcasted_iota(jnp.int32, (8, chunk), 1)
    offsets = jnp.zeros((8, chunk), jnp.float32)
    for h in range(heads):
        offsets = jnp.where(head_row == h, off_ref[mine * heads + h], offsets)
    dec_rows = jnp.zeros((16, width), jnp.float32)
    for b in range(seqs):
        query = jnp.where(own_head, dq_ref[b : b + 1, :].astype(jnp.float32), 0.0).astype(jnp.bfloat16)
        out, unused = cached_terms(
            query,
            lambda start: dk_ref[b, pl.ds(start, chunk), :],
            lambda start: dv_ref[b, pl.ds(start, chunk), :],
            lambda start: jnp.where(spot + start < len_ref[b], offsets, HIDDEN),
            slots, chunk, suffix, scale,
        )
        line = jnp.sum(jnp.where(own_head, out, 0.0), axis=0, keepdims=True)
        place = lax.broadcasted_iota(jnp.int32, (16, width), 0)
        dec_rows = jnp.where(place == b, line, dec_rows)
    for p in range(parts):
        att[p, pl.ds(rows, 16), :] = dec_rows[:, p * band : p * band + band].astype(att.dtype)

    if far:
        for p in range(parts):
            forward_q(3, p)

    def later_step(t, carry):
        step(t, carry)

        @pl.when(t == parts + KV_AT)
        def _():
            for s in range(1, nz):
                forward_kv(s)

        return carry

    lax.fori_loop(parts, nz * parts, later_step, 0)
    pieces()

    def tail(t, carry):
        combine(*place_of(t))
        return carry

    lax.fori_loop(nz * parts - LAG, nz * parts, tail, 0)

    for h in range(heads):
        plane = lax.rem(z, halves) * heads + h

        @pl.when(plane != z)
        def _():
            remote(ps.at[0], pr.at[h], p_s.at[0], p_r.at[h], plane * ny + y).wait_recv()
            remote(pt.at[0], ptr.at[h], pt_s.at[0], pt_r.at[h], plane * ny + y).wait_recv()

    core = lax.rem(mine, 2)
    sibling = mine + 1 - 2 * core

    def across(s, p):
        return remote(att.at[p], attg.at[mine, p], a_s.at[s, p], a_r.at[mine, p], lax.rem(mine + 2 * s, tp), "tp")

    def aside(p):
        return remote(att.at[p], attg.at[mine, p], a_s.at[0, p], a_r.at[mine, p], sibling, "tp")

    def beside(c, p):
        return remote(attg.at[c, p], attg.at[c, p], b_s.at[c, p], a_r.at[c, p], sibling, "tp")

    for p in range(parts):
        for s in range(1, nz):
            o_plane(s, p).wait_recv()
            t_plane(s, p).wait_recv()
        mine_left, near_left = zmine[p], ztr[0, p]
        scales = [jnp.where(even, near_left, one), jnp.where(even, one, mine_left)]
        if far:
            low = z < 2
            beyond = jnp.where(low, ztr[1, p] * ztr[2, p], one)
            nearer = jnp.where(low, one, mine_left * near_left)
            scales = [x * beyond for x in scales]
            scales.append(jnp.where(even, ztr[2, p], one) * nearer)
            scales.append(jnp.where(even, one, ztr[1, p]) * nearer)
        for h in range(share):
            line = slice(h, h + 1)
            total = zmix[p, head_cols(h), :] * scales[0][line, :]
            for s in range(1, nz):
                total += zr[s - 1, p, head_cols(h), :].astype(jnp.float32) * scales[s][line, :]
            head = p * share + h
            total = total * ptr[head, 0:1, :] + pr[head].astype(jnp.float32)
            att[p, pl.ds(0, rows), head_cols(h)] = jnp.transpose(total).astype(att.dtype)
        for s in range(1, tp // 2):
            across(s, p).start()
        aside(p).start()
        attg[mine, p] = att[p]

    for p in range(parts):
        for s in direct:
            q_plane(s, p).wait_send()
        if far:
            q_relay(2, p).wait_send()
        for s in range(1, nz):
            o_plane(s, p).wait_send()
            t_plane(s, p).wait_send()
            for k in range(1, ny):
                q_block(source(s) * ny + y, s, p, k).wait_send()
        for k in range(1, ny):
            q_column(k, p).wait_send()
            for s in range(nz):
                o_column(source(s), s, p, k).wait_send()
                t_column(source(s), s, p, k).wait_send()
    for s in range(1, nz):
        for k in range(1, ny):
            kv_block(source(s) * ny + y, s, k).wait_send()
    for k in range(1, ny):
        kv_column(k).wait_send()
    for t in range(nz):
        pl.when(z != t)(lambda t=t: kv_plane(t).wait_send())
    for j in range(heads):

        @pl.when(my_part + halves * j != z)
        def _():
            piece_out(j).wait_send()
            piece_total(j).wait_send()

    for p in range(parts):
        for s in range(1, tp // 2):
            c = lax.rem(mine + tp - 2 * s, tp)
            beside(c, p).wait_recv()
            beside(c, p).start()
    for p in range(parts):
        for s in range(tp // 2):
            beside(lax.rem(sibling + 2 * s, tp), p).wait_recv()
        aside(p).wait_send()
        for s in range(1, tp // 2):
            across(s, p).wait_send()
            beside(lax.rem(mine + tp - 2 * s, tp), p).wait_send()
    square = jnp.zeros((rows + 16, 1), jnp.float32)
    for t in range(tp):
        for p in range(parts):
            values = attg[t, p].astype(jnp.float32)
            square += jnp.sum(values * values, axis=-1, keepdims=True)
    inverse = lax.rsqrt(square / (tp * width) + EPS)
    gain_out = gain_ref[...].astype(jnp.float32)[None, :]
    for t in range(tp):
        for p in range(parts):
            cols = slice(t * width + p * band, t * width + p * band + band)
            normed[:, cols] = (attg[t, p].astype(jnp.float32) * inverse * gain_out[:, cols]).astype(jnp.bfloat16)
    load_out.wait()
    result = dot(normed[...], wo_ref[...]).astype(jnp.bfloat16)
    out_ref[...] = result[0:rows]
    dec_ref[...] = result[rows : rows + seqs]
    for keep in keeps:
        keep.wait()


def deliver_kernel(*refs):
    sems = refs[-1]
    count = sems.shape[1]
    sources, targets, held = refs[:count], refs[count : 2 * count], refs[2 * count : 3 * count]
    taken = [pltpu.make_async_copy(sources[i], held[i], sems.at[0, i]) for i in range(count)]
    given = [pltpu.make_async_copy(held[i], targets[i], sems.at[1, i]) for i in range(count)]
    for i in range(count):
        taken[i].start()
    for i in range(count):
        taken[i].wait()
        given[i].start()
    for i in range(count):
        given[i].wait()


def body(
    piece_tokens, decode_tokens, norm_gain, w_query, w_key, w_value, score_offset, context_length,
    prompt_keys, prompt_values, decode_keys, decode_values, decoding_cache_length, out_gain, w_out,
):
    n, tp = lax.axis_size("kv"), lax.axis_size("tp")
    nz, ny = grid_of(n)
    rows, model = piece_tokens.shape
    width = w_query.shape[1]
    seqs = decode_keys.shape[0]
    heads = width // HEAD
    assert nz % heads == 0 and tp % 2 == 0 and nz in (2, 4)
    parts = 2 if heads % 2 == 0 else 1
    share, band = heads // parts, width // parts
    cache_rows = prompt_keys.shape[0]
    vmem = pl.BlockSpec(memory_space=pltpu.VMEM)
    smem = pl.BlockSpec(memory_space=pltpu.SMEM)
    hbm = pl.BlockSpec(memory_space=pl.ANY)
    dma = pltpu.SemaphoreType.DMA

    def half(*shape):
        return pltpu.VMEM(shape, jnp.bfloat16)

    def full(*shape):
        return pltpu.VMEM(shape, jnp.float32)

    def result(*shape):
        return jax.ShapeDtypeStruct(shape, jnp.bfloat16)

    results = pl.pallas_call(
        functools.partial(attention_kernel, nz, ny, tp, heads, parts),
        out_shape=(
            result(rows, w_out.shape[1]), result(seqs, w_out.shape[1]), result(rows, width), result(rows, width),
            result(seqs, width), result(seqs, width),
        ),
        in_specs=[hbm] * 10 + [vmem] * 2 + [smem] * 3,
        out_specs=(vmem, vmem, hbm, hbm, vmem, vmem),
        scratch_shapes=[
            half(rows, model), half(seqs, model), half(model, width), half(model, width), half(model, width),
            half(*prompt_keys.shape), half(*prompt_values.shape), half(*decode_keys.shape), half(*decode_values.shape),
            half(*w_out.shape),
            half(rows + 16, model), half(parts, rows, band), half(rows, width), half(rows, width), half(16, width),
            half(rows + 16, tp * width),
            half(n, parts, rows, band), half(heads, cache_rows, HEAD), half(heads, HEAD, cache_rows),
            full(heads, cache_rows, 128), full(share, cache_rows, ny * rows),
            full(nz, parts, ny, band, rows), half(nz, parts, ny, band, rows), full(nz, parts, ny, 8, 128),
            half(nz, parts, ny, band, rows), full(nz, parts, ny, 8, 128), full(ny, band, rows), full(band, rows),
            half(nz, parts, band, rows), full(nz, parts, 8, 128), half(nz, parts, band, rows),
            full(nz, parts, 8, 128), full(parts, band, rows), full(parts, 8, 128),
            half(heads, 2 * rows, HEAD), half(n, 2 * rows, HEAD), half(heads * rows, HEAD),
            full(4, rows, heads * rows), full(4, HEAD, heads * rows), full(HEAD, heads * rows), full(8, heads * rows),
            half(heads, HEAD, rows), full(heads, 8, 128), half(heads, HEAD, rows), full(heads, 8, 128),
            half(parts, rows + 16, band), half(tp, parts, rows + 16, band),
            dma((ny, parts)), dma((nz, parts)), dma((nz, parts, ny)), dma((n, parts)),
            dma((nz,)), dma((ny,)), dma((nz, ny)), dma((n,)),
            dma((nz, parts, ny)), dma((nz, parts, ny)), dma((nz, parts, ny)), dma((nz, parts, ny)),
            dma((nz, parts)), dma((nz, parts)), dma((nz, parts)), dma((nz, parts)),
            dma((heads,)), dma((heads,)), dma((heads,)), dma((heads,)),
            dma((tp, parts)), dma((tp, parts)), dma((tp, parts)), dma((7,)), dma((3, 8)), dma((2,)),
            dma((parts,)),
        ],
        compiler_params=pltpu.CompilerParams(
            collective_id=0, has_side_effects=True, vmem_limit_bytes=60 * 1024 * 1024
        ),
        name="attend",
    )(
        piece_tokens, decode_tokens, w_query, w_key, w_value, prompt_keys, prompt_values, decode_keys, decode_values,
        w_out, norm_gain, out_gain, score_offset, context_length, decoding_cache_length,
    )
    kinds = [jax.ShapeDtypeStruct(r.shape, r.dtype) for r in results]
    return pl.pallas_call(
        deliver_kernel,
        out_shape=kinds,
        in_specs=[hbm] * len(kinds),
        out_specs=[hbm] * len(kinds),
        scratch_shapes=[pltpu.VMEM(k.shape, k.dtype) for k in kinds] + [dma((2, len(kinds)))],
        name="deliver",
    )(*results)


def solution(mesh):
    in_specs = (
        P("kv", None),
        P("kv", None),
        P(),
        P(None, "tp"),
        P(None, "tp"),
        P(None, "tp"),
        P(),
        P(),
        P("kv", "tp"),
        P("kv", "tp"),
        P("kv", None, "tp"),
        P("kv", None, "tp"),
        P("kv"),
        P(),
        P(None, "tp"),
    )
    out_specs = (
        P("kv", "tp"),
        P("kv", "tp"),
        P("kv", "tp"),
        P("kv", "tp"),
        P("kv", "tp"),
        P("kv", "tp"),
    )
    return jax.shard_map(body, mesh=mesh, in_specs=in_specs, out_specs=out_specs, check_vma=False)
```

time: 64.1 us -> 60.4 us (0.942)
  the two profiles are of different devices: /device:TPU:9 before, /device:TPU:0 now
where the time goes in v3:
time: 60.4 us; the launch traced here: 60.1 us
  Pallas kernels  58.2 us (96%)
  between operations  1.94 us (3%)
    pallas_call x1, Pallas kernels, body(): pl.pallas_call(functools.partial(attention_kernel, nz, ny, tp, heads, par...  56.3 us
    pallas_call x1, Pallas kernels, body(): pl.pallas_call(deliver_kernel, out_shape=kinds, in_specs=[hbm] * len(kind...  1.85 us

profile of v3, /device:TPU:0, one launch (start us, length us, event | category | flops | bytes accessed | tf_op | source)
XLA Modules:
  0.0 60.1 jit_solution(5154424572788300103)
XLA Ops:
  1.9 56.3 %attend.1 = (bf16[128,1024]{1,0:T(8,128)(2,1)}, bf16[1,1024]{1,0:T(2,128)(2,1)}, bf16[128,512]{1,0:T(8,128)(2,1)}, bf16[128,512]{1,0:T(8,128)(2,1)}, bf16[1,512]{1,0:T(2,128)(2,1)}, /*index=5*/bf16[1,512]{1,0:T(2,128)(2,1)}) custom-call(bf16[128,4096]{1,0:T(8,128)(2,1)} %x_hbm.1, bf16[1,4096]{1,0:T(2,128)(2,1)} %d_hbm.1, bf16[4096,512]{1,0:T(8,128)(2,1)} %wq_hbm.1, ...), custom_call_target="tpu_custom_call" | custom-call | tf_op jit(solution)/shard_map/attend/pallas_call | solution.py:671
  58.3 1.8 %deliver.1 = (bf16[128,1024]{1,0:T(8,128)(2,1)}, bf16[1,1024]{1,0:T(2,128)(2,1)}, bf16[128,512]{1,0:T(8,128)(2,1)}, bf16[128,512]{1,0:T(8,128)(2,1)}, bf16[1,512]{1,0:T(2,128)(2,1)}, /*index=5*/bf16[1,512]{1,0:T(2,128)(2,1)}) custom-call(bf16[128,1024]{1,0:T(8,128)(2,1)} %get-tuple-element.12.refs_0_, bf16[1,1024]{1,0:T(2,128)(2,1)} %get-tuple-element.13.refs_1_, ...), custom_call_target="tpu_custom_call" | custom-call | tf_op jit(solution)/shard_map/deliver/pallas_call | solution.py:712
